TPU v7x, 1024 devices: a whole 4x8x16 slice. The times are simulated.
1024 devices in a mesh: sp: 128 (over z, y), tp: 8 (over x, core).
Axes of the slice: x: 4, y: 8, z: 16, core: 2. Of those that a mesh axis runs over, the one named last changes fastest.
Arguments:
- glu_value: bfloat16 [65536, 1024], P('sp', 'tp'), may hold values from -6 to 6
- glu_gate: bfloat16 [65536, 1024], P('sp', 'tp'), may hold values from -8 to 8
- conv_taps: bfloat16 [31, 1024], P(None, 'tp'), may hold values from -1 to 1
- norm_gain: float32 [1024], P('tp'), may hold values from 0.1 to 1.9
- out_weight: bfloat16 [2048, 1024], P(None, 'tp'), may hold values from -0.1875 to 0.1875
- norm_mean: float32 [65536], P('sp'), may hold values from -3 to 3
- norm_scale: float32 [65536], P('sp'), may hold values from 0.5 to 2
- out_grad: bfloat16 [65536, 2048], P('sp'), may hold values from -24 to 24
Outputs:
- value_grad: bfloat16 [65536, 1024], P('sp', 'tp')
- gate_grad: bfloat16 [65536, 1024], P('sp', 'tp')
- taps_grad: float32 [31, 1024], P(None, 'tp')
- gain_grad: float32 [1024], P('tp')
- weight_grad: float32 [2048, 1024], P('sp', 'tp')
All inputs are finite; a program needn't handle non-finite values.
Results may differ from a plain program's by a relative error of at most 0.0047.
Values may be sent and summed in bfloat16 or wider, within the bound.
No kernel may reach another device: no remote copies, remote signals or barrier semaphores. Data moves between devices by JAX's collectives and lax.ppermute only.
A program may use at most 32 MiB of HBM per device.

v0:
```python
import jax
import jax.numpy as jnp
from jax import lax
from jax.sharding import Mesh
from jax.sharding import PartitionSpec as P

CH = 1024
SP = ("sp_0", "sp_1")


def passed_along(value, axis, by):
    length = lax.axis_size(axis)
    pairs = [(i, i + by) for i in range(length) if 0 <= i + by < length]
    return lax.ppermute(value, axis, pairs)


def from_everyone(value, axis):
    copies = jnp.broadcast_to(value, (lax.axis_size(axis), *value.shape))
    return lax.all_to_all(copies, axis, split_axis=0, concat_axis=0, tiled=True)


def of_everyone(value, axis):
    return from_everyone(value, axis).sum(axis=0)


def in_one(arrays, axis):
    ends = [0]
    for a in arrays:
        ends.append(ends[-1] + a.size)
    so_far = of_everyone(jnp.concatenate([a.ravel() for a in arrays]), axis)
    return tuple((so_far[b:e].reshape(a.shape) for a, b, e in zip(arrays, ends, ends[1:])))


def sum_by_axis(so_far, axes):
    for axis in axes:
        so_far = lax.psum_scatter(so_far, axis, scatter_dimension=0, tiled=True)
    return so_far


def by_axis(value, axes):
    for axis in axes:
        value = lax.psum(value, axis)
    return value


def per_device(
    glu_value, glu_gate, conv_taps, norm_gain, out_weight, norm_mean, norm_scale, out_grad
):
    tok_rows = glu_value.shape[0]
    reach_back = conv_taps.shape[0] - 1
    val_float = glu_value.astype(jnp.float32)
    gate_sig = jax.nn.sigmoid(glu_gate.astype(jnp.float32))
    gated = (val_float * gate_sig).astype(jnp.bfloat16)
    before = passed_along(gated[tok_rows - reach_back :], SP, 1)
    padded = jnp.concatenate([before, gated], axis=0).astype(jnp.float32)
    taps_float = conv_taps.astype(jnp.float32)
    conv = jnp.zeros(gated.shape, jnp.float32)
    for offset in range(reach_back + 1):
        conv = conv + taps_float[offset] * padded[offset : offset + tok_rows]
    centered = (conv - norm_mean[:, None]) * norm_scale[:, None]
    normed = centered * norm_gain
    sig_norm = jax.nn.sigmoid(normed)
    activated = (normed * sig_norm).astype(jnp.bfloat16)
    act_grad = jnp.dot(out_grad, out_weight, preferred_element_type=jnp.float32)
    normed_grad = act_grad * sig_norm * (1.0 + normed * (1.0 - sig_norm))
    gain_local = jnp.sum(normed_grad * centered, axis=0)
    scaled_grad = normed_grad * norm_gain
    sum_plain, sum_cross = in_one(
        (jnp.sum(scaled_grad, axis=1), jnp.sum(scaled_grad * centered, axis=1)), "tp"
    )
    mean_plain = sum_plain / CH
    mean_cross = sum_cross / CH
    conv_grad = norm_scale[:, None] * (
        scaled_grad - mean_plain[:, None] - centered * mean_cross[:, None]
    )
    after = passed_along(conv_grad[:reach_back], SP, -1)
    grad_padded = jnp.concatenate([conv_grad, after], axis=0)
    gated_grad = jnp.zeros(conv_grad.shape, jnp.float32)
    tap_list = []
    for offset in range(reach_back + 1):
        begin = reach_back - offset
        gated_grad = gated_grad + taps_float[offset] * grad_padded[begin : begin + tok_rows]
        tap_list.append(jnp.sum(conv_grad * padded[offset : offset + tok_rows], axis=0))
    taps_local = jnp.stack(tap_list, axis=0)
    value_grad = (gated_grad * gate_sig).astype(jnp.bfloat16)
    gate_grad = (gated_grad * val_float * gate_sig * (1.0 - gate_sig)).astype(jnp.bfloat16)
    weight_grad = sum_by_axis(
        lax.dot_general(
            out_grad, activated, (((0,), (0,)), ((), ())), preferred_element_type=jnp.float32
        ),
        SP,
    )
    taps_grad, gain_grad = (by_axis(taps_local, SP), by_axis(gain_local, SP))
    return (value_grad, gate_grad, taps_grad, gain_grad, weight_grad)


def solution(mesh):
    torus = Mesh(mesh.devices.reshape(16, 8, mesh.shape["tp"]), ("sp_0", "sp_1", "tp"))
    placed = (
        P(SP, "tp"),
        P(SP, "tp"),
        P(None, "tp"),
        P("tp"),
        P(None, "tp"),
        P(SP),
        P(SP),
        P(SP, None),
    )
    return jax.shard_map(
        per_device,
        mesh=torus,
        in_specs=placed,
        out_specs=(P(SP, "tp"), P(SP, "tp"), P(None, "tp"), P("tp"), P(SP, "tp")),
        check_vma=False,
    )
```

profile of v0, /device:TPU:8, one launch (start us, length us, event | category | flops | bytes accessed | tf_op | source)
XLA Modules:
  0.0 178.9 jit_solution(16155667362896455874)
XLA Ops:
  7.2 0.0 copy-start
  7.2 0.0 reduce-scatter.5.cloned.1.call-start
  7.2 1.2 fusion.1
  8.4 3.5 %collective-permute-start = (bf16[30,128]{1,0:T(8,128)(2,1)S(1)}, bf16[30,128]{1,0:T(8,128)(2,1)S(1)}, u32[]{:S(2)}, u32[]{:S(2)}) collective-permute-start(bf16[30,128]{1,0:T(8,128)(2,1)S(1)} %slice.447), channel_id=1, source_target_pairs={{0,8},{8,16},{16,24},{24,32},{32,40},{40,48},{48,56},{56,64},{64,7... | collective-permute-start | bytes 23048 | tf_op jit(solution)/shard_map/ppermute | solution.py:14
  11.9 0.7 convert_element_type.24
  12.7 11.8 %collective-permute-done = bf16[30,128]{1,0:T(8,128)(2,1)S(1)} collective-permute-done((bf16[30,128]{1,0:T(8,128)(2,1)S(1)}, bf16[30,128]{1,0:T(8,128)(2,1)S(1)}, u32[]{:S(2)}, u32[]{:S(2)}) %collective-permute-start) | collective-permute-done | bytes 7712 | tf_op jit(solution)/shard_map/ppermute | solution.py:14
  24.4 0.0 copy-start.5
  24.5 1.5 subtract_multiply_fusion.1
  25.9 0.0 copy-done
  25.9 0.0 copy-done.5
  26.0 1.5 convolution_bitcast_fusion
  27.5 0.0 reduce-scatter.5.cloned.1.call-update
  27.5 0.0 copy-start.3
  27.5 0.0 copy-start.4
  27.5 0.0 reduce-scatter.7.cloned.1.call-start
  27.6 1.9 %multiply_reduce_fusion = (f32[128]{0:T(128)S(1)}, f32[512]{0:T(512)S(1)}, f32[512]{0:T(512)S(1)}, f32[512,128]{1,0:T(8,128)S(1)}) fusion(f32[512,128]{1,0:T(8,128)S(1)} %subtract_multiply_fusion.1, f32[128]{0:T(128)S(1)} %copy-done.5, bf16[512,2048]{1,0:T(8,128)(2,1)S(1)} %copy-done, bf16[2048,128]{1,0:T(8,128)(2,1)} %param.12), kind=kOutput, calls=%fused_computation.146 | convolution fusion | flops 269417344 | bytes 3150848 | tf_op jit(solution)/shard_map/dot_general | solution.py:64
  29.5 7.8 %all_to_all.6 = f32[8,1,1024]{2,1,0:T(1,128)S(1)} all-to-all(f32[8,1,1024]{2,1,0:T(1,128)S(1)} %broadcast_in_dim.2), channel_id=1, replica_groups=mesh['sp_0'=16,'sp_1'=8,'tp'=8] {'tp'}, dimensions={0} | all-to-all | bytes 65536 | tf_op jit(solution)/shard_map/all_to_all | solution.py:19
  37.3 0.0 copy-done.3
  37.3 0.0 copy-done.4
  37.4 2.2 %multiply_reduce_fusion.1 = (f32[128]{0:T(128)S(1)}, f32[128]{0:T(128)S(1)}, f32[128]{0:T(128)S(1)}, f32[128]{0:T(128)S(1)}, f32[128]{0:T(128)S(1)}, /*index=5*/...) fusion(f32[542,128]{1,0:T(8,128)S(1)} %maximum_convert_fusion, ...), kind=kLoop, calls=%fused_computation.147 | loop fusion | flops 6813440 | bytes 8684544 | tf_op jit(solution)/shard_map/reduce_sum | solution.py:83
  39.6 0.0 copy-start.1
  39.6 0.0 copy-start.2
  39.6 2.1 %collective-permute-start.1 = (f32[30,128]{1,0:T(8,128)S(1)}, f32[30,128]{1,0:T(8,128)S(1)}, u32[]{:S(2)}, u32[]{:S(2)}) collective-permute-start(f32[30,128]{1,0:T(8,128)S(1)} %slice.509), channel_id=1, source_target_pairs={{8,0},{16,8},{24,16},{32,24},{40,32},{48,40},{56,48},{64,56},{72,6... | collective-permute-start | bytes 46088 | tf_op jit(solution)/shard_map/ppermute | solution.py:14
  41.7 0.4 multiply_reduce_fusion.19
  42.0 0.1 stack.127
  42.1 62.8 %all-reduce = (f32[31,128]{1,0:T(8,128)S(1)}, f32[128]{0:T(128)S(1)}) all-reduce(f32[31,128]{1,0:T(8,128)S(1)} %stack.127, f32[128]{0:T(128)S(1)} %get-tuple-element.56), channel_id=1, replica_groups=mesh['sp_0'=16,'sp_1'=8,'tp'=8] {'sp_0'}, use_global_device_ids=true, to_apply=%region_34.0 | all-reduce | flops 4096 | bytes 32768 | tf_op jit(solution)/shard_map/psum | solution.py:42
  104.9 27.6 %all-reduce.1 = (f32[31,128]{1,0:T(8,128)}, f32[128]{0:T(128)}) all-reduce(f32[31,128]{1,0:T(8,128)S(1)} %get-tuple-element.59, f32[128]{0:T(128)S(1)} %get-tuple-element.60), channel_id=1, replica_groups=mesh['sp_0'=16,'sp_1'=8,'tp'=8] {'sp_1'}, use_global_device_ids=true, to_apply=%region_35.0 | all-reduce | flops 4096 | bytes 32768 | tf_op jit(solution)/shard_map/psum | solution.py:42
  132.4 0.0 collective-permute-done.1
  132.4 0.0 copy-done.1
  132.4 0.0 copy-done.2
  132.4 1.6 fusion.4
  134.1 0.0 reduce-scatter.5.cloned.1.call-done
  134.1 1.6 copy.18
  135.6 0.0 reduce-scatter.7.cloned.1.call-update
  135.6 0.7 multiply_convert_fusion.1
  136.4 35.7 %reduce-scatter.7.cloned.1.call-done = f32[16,128]{1,0:T(8,128)} async-done(((f32[128,128]{1,0:T(8,128)}), f32[16,128]{1,0:T(8,128)}) %reduce-scatter.7.cloned.1.call-update) | async-done | bytes 8208
  (9 shorter events, 0.1 us)
Async XLA Ops:
  7.2 18.8 %copy-start = (bf16[512,2048]{1,0:T(8,128)(2,1)S(1)}, bf16[512,2048]{1,0:T(8,128)(2,1)}, u32[]{:S(2)}) copy-start(bf16[512,2048]{1,0:T(8,128)(2,1)} %param.15) | copy-start | bytes 6291460
  7.2 126.9 %reduce-scatter.5.cloned.1.call-start = ((), (), s32[]{:S(2)}) async-start(), calls=%async_computation.3 | async-start | bytes 1114112 | tf_op jit(solution)/shard_map/reduce_scatter | solution.py:36
  8.4 16.0 %collective-permute-start = (bf16[30,128]{1,0:T(8,128)(2,1)S(1)}, bf16[30,128]{1,0:T(8,128)(2,1)S(1)}, u32[]{:S(2)}, u32[]{:S(2)}) collective-permute-start(bf16[30,128]{1,0:T(8,128)(2,1)S(1)} %slice.447), channel_id=1, source_target_pairs={{0,8},{8,16},{16,24},{24,32},{32,40},{40,48},{48,56},{56,64},{64,7... | collective-permute-start | bytes 23048 | tf_op jit(solution)/shard_map/ppermute | solution.py:14
  24.4 1.5 copy-start.5
  27.5 9.8 %copy-start.3 = (f32[512]{0:T(512)S(1)}, f32[512]{0:T(512)}, u32[]{:S(2)}) copy-start(f32[512]{0:T(512)} %param.13) | copy-start | bytes 6148
  27.5 9.8 %copy-start.4 = (f32[512]{0:T(512)S(1)}, f32[512]{0:T(512)}, u32[]{:S(2)}) copy-start(f32[512]{0:T(512)} %param.14) | copy-start | bytes 6148
  27.5 144.6 %reduce-scatter.7.cloned.1.call-start = ((), (), s32[]{:S(2)}) async-start(), calls=%async_computation.4 | async-start | bytes 73728
  39.6 92.9 %copy-start.1 = (bf16[512,128]{1,0:T(8,128)(2,1)S(1)}, bf16[512,128]{1,0:T(8,128)(2,1)}, u32[]{:S(2)}) copy-start(bf16[512,128]{1,0:T(8,128)(2,1)} %param.9) | copy-start | bytes 393220
  39.6 92.9 %copy-start.2 = (bf16[512,128]{1,0:T(8,128)(2,1)S(1)}, bf16[512,128]{1,0:T(8,128)(2,1)}, u32[]{:S(2)}) copy-start(bf16[512,128]{1,0:T(8,128)(2,1)} %param.8) | copy-start | bytes 393220
  39.6 92.8 %collective-permute-start.1 = (f32[30,128]{1,0:T(8,128)S(1)}, f32[30,128]{1,0:T(8,128)S(1)}, u32[]{:S(2)}, u32[]{:S(2)}) collective-permute-start(f32[30,128]{1,0:T(8,128)S(1)} %slice.509), channel_id=1, source_target_pairs={{8,0},{16,8},{24,16},{32,24},{40,32},{48,40},{56,48},{64,56},{72,6... | collective-permute-start | bytes 46088 | tf_op jit(solution)/shard_map/ppermute | solution.py:14
Sparse Core Ops, SparseCore 0:
  27.6 74.1 reduce-scatter.4
  135.8 36.2 reduce-scatter.6
where the time goes:
time: 179 us
  blocking collectives  98.1 us (55%)
  waiting for transfers between devices  47.5 us (27%)
  between operations  14.2 us (8%)
  other arithmetic  8.36 us (5%)
  starting transfers between devices  5.62 us (3%)
  matrix products  3.37 us (2%)
    psum x2, blocking collectives, by_axis(): value = lax.psum(value, axis)  90.3 us
    unnamed x3, waiting for transfers between devices  35.7 us
    ppermute x2, waiting for transfers between devices, passed_along(): return lax.ppermute(value, axis, pairs)  11.8 us
    all_to_all x1, blocking collectives, from_everyone(): return lax.all_to_all(copies, axis, split_axis=0, concat_axis=0, tiled=True)  7.82 us
    ppermute x2, starting transfers between devices, passed_along(): return lax.ppermute(value, axis, pairs)  5.54 us
  transfers between devices with their start and end apart: 4, of which 2 were waited for; matrix products, arithmetic and copies ran while one was open for 4% of the time, Pallas kernels for 0%

commit v1 on v0

v1 whole, which is shorter than its diff:
```python
import jax
import jax.numpy as jnp
from jax import lax
from jax.sharding import Mesh
from jax.sharding import PartitionSpec as P

CH = 1024
SP = ("z", "y")


def passed_along(value, axis, by):
    length = lax.axis_size(axis)
    pairs = [(i, i + by) for i in range(length) if 0 <= i + by < length]
    return lax.ppermute(value, axis, pairs)


def exchange(value, axis):
    return lax.all_to_all(value, axis, split_axis=0, concat_axis=0, tiled=True)


def to_all(value, axis):
    copies = jnp.broadcast_to(value, (lax.axis_size(axis), *value.shape))
    return exchange(copies, axis)


def per_device(
    glu_value, glu_gate, conv_taps, norm_gain, out_weight, norm_mean, norm_scale, out_grad
):
    f32, bf16 = jnp.float32, jnp.bfloat16
    tok_rows, chans = glu_value.shape
    reach_back = conv_taps.shape[0] - 1
    n_z, n_y = lax.axis_size("z"), lax.axis_size("y")
    val_float = glu_value.astype(f32)
    gate_sig = jax.nn.sigmoid(glu_gate.astype(f32))
    gated = (val_float * gate_sig).astype(bf16)
    before = passed_along(gated[tok_rows - reach_back :], SP, 1)
    padded = jnp.concatenate([before, gated], axis=0).astype(f32)
    taps_float = conv_taps.astype(f32)
    conv = jnp.zeros(gated.shape, f32)
    for offset in range(reach_back + 1):
        conv = conv + taps_float[offset] * padded[offset : offset + tok_rows]
    centered = (conv - norm_mean[:, None]) * norm_scale[:, None]
    normed = centered * norm_gain
    sig_norm = jax.nn.sigmoid(normed)
    activated = (normed * sig_norm).astype(bf16)
    act_grad = jnp.dot(out_grad, out_weight, preferred_element_type=f32)
    normed_grad = act_grad * sig_norm * (1.0 + normed * (1.0 - sig_norm))
    gain_local = jnp.sum(normed_grad * centered, axis=0)
    scaled_grad = normed_grad * norm_gain
    sums = jnp.stack([jnp.sum(scaled_grad, axis=1), jnp.sum(scaled_grad * centered, axis=1)])
    sums = to_all(sums.reshape(1, -1), "tp").sum(axis=0).reshape(2, tok_rows)
    mean_plain = sums[0] / CH
    mean_cross = sums[1] / CH
    weight_part = lax.dot_general(
        out_grad, activated, (((0,), (0,)), ((), ())), preferred_element_type=f32
    )
    own_rows = weight_part.shape[0] // (n_z * n_y)
    weight_part = weight_part.astype(bf16).reshape(n_z, n_y, own_rows, chans)
    weight_part = weight_part.transpose(1, 0, 2, 3).reshape(n_y, n_z * own_rows, chans)
    weight_part = exchange(weight_part, "y").astype(f32).sum(axis=0)

    conv_grad = norm_scale[:, None] * (
        scaled_grad - mean_plain[:, None] - centered * mean_cross[:, None]
    )
    after = passed_along(conv_grad[:reach_back], SP, -1)
    grad_padded = jnp.concatenate([conv_grad, after], axis=0)
    gated_grad = jnp.zeros(conv_grad.shape, f32)
    tap_list = []
    for offset in range(reach_back + 1):
        begin = reach_back - offset
        gated_grad = gated_grad + taps_float[offset] * grad_padded[begin : begin + tok_rows]
        tap_list.append(jnp.sum(conv_grad * padded[offset : offset + tok_rows], axis=0))
    small = jnp.stack([*tap_list, gain_local], axis=0)
    small = to_all(small, "y").sum(axis=0).astype(bf16)
    value_grad = (gated_grad * gate_sig).astype(bf16)
    gate_grad = (gated_grad * val_float * gate_sig * (1.0 - gate_sig)).astype(bf16)

    last = jnp.concatenate(
        [
            weight_part.astype(bf16).reshape(n_z, own_rows, chans),
            jnp.broadcast_to(small, (n_z, *small.shape)),
        ],
        axis=1,
    )
    last = exchange(last, "z").astype(f32).sum(axis=0)
    weight_grad = last[:own_rows]
    taps_grad = last[own_rows : own_rows + reach_back + 1]
    gain_grad = last[own_rows + reach_back + 1]
    return (value_grad, gate_grad, taps_grad, gain_grad, weight_grad)


def solution(mesh):
    torus = Mesh(mesh.devices.reshape(16, 8, mesh.shape["tp"]), ("z", "y", "tp"))
    placed = (
        P(SP, "tp"),
        P(SP, "tp"),
        P(None, "tp"),
        P("tp"),
        P(None, "tp"),
        P(SP),
        P(SP),
        P(SP, None),
    )
    return jax.shard_map(
        per_device,
        mesh=torus,
        in_specs=placed,
        out_specs=(P(SP, "tp"), P(SP, "tp"), P(None, "tp"), P("tp"), P(SP, "tp")),
        check_vma=False,
    )
```

time: 179 us -> 96.3 us (0.54)
  the two profiles are of different devices: /device:TPU:8 before, /device:TPU:2 now
where the time goes in v1:
time: 96.3 us; the launch traced here: 95.7 us
  waiting for transfers between devices  34.1 us (35%)
  starting transfers between devices  27.4 us (28%)
  blocking collectives  17.3 us (18%)
  other arithmetic  9.17 us (10%)
  local copies, waits for them, and re-layouts  4.73 us (5%)
  matrix products  2.13 us (2%)
    all_to_all x3, waiting for transfers between devices, exchange(): return lax.all_to_all(value, axis, split_axis=0, concat_axis=0, tiled=True)  29.1 us
    all_to_all x3, starting transfers between devices, exchange(): return lax.all_to_all(value, axis, split_axis=0, concat_axis=0, tiled=True)  22.7 us
    all_to_all x1, blocking collectives, exchange(): return lax.all_to_all(value, axis, split_axis=0, concat_axis=0, tiled=True)  17.3 us
    ppermute x2, waiting for transfers between devices, passed_along(): return lax.ppermute(value, axis, pairs)  4.95 us
    ppermute x2, starting transfers between devices, passed_along(): return lax.ppermute(value, axis, pairs)  4.77 us
    reduce_sum x2, other arithmetic, per_device(): jnp.sum(conv_grad * padded[offset:offset + tok_rows], axis=0)  2.56 us
  transfers between devices with their start and end apart: 5, of which 5 were waited for; matrix products, arithmetic and copies ran while one was open for 7% of the time, Pallas kernels for 0%

profile of v1, /device:TPU:2, one launch (start us, length us, event | category | flops | bytes accessed | tf_op | source)
XLA Modules:
  0.0 95.7 jit_solution(5816734258983084579)
XLA Ops:
  0.6 0.0 copy-start
  0.6 1.2 %fusion.2 = bf16[512,128]{1,0:T(8,128)(2,1)S(1)} fusion(bf16[512,128]{1,0:T(8,128)(2,1)} %param.8, bf16[512,128]{1,0:T(8,128)(2,1)} %param.9), kind=kLoop, calls=%fused_computation.36 | loop fusion | flops 458752 | bytes 393216 | tf_op jit(solution)/shard_map/convert_element_type | solution.py:35
  1.9 3.5 %collective-permute-start = (bf16[30,128]{1,0:T(8,128)(2,1)S(1)}, bf16[30,128]{1,0:T(8,128)(2,1)S(1)}, u32[]{:S(2)}, u32[]{:S(2)}) collective-permute-start(bf16[30,128]{1,0:T(8,128)(2,1)S(1)} %slice.461), channel_id=1, source_target_pairs={{0,8},{8,16},{16,24},{24,32},{32,40},{40,48},{48,56},{56,64},{64,7... | collective-permute-start | bytes 23048 | tf_op jit(solution)/shard_map/ppermute | solution.py:14
  5.3 0.7 convert_element_type.38
  6.1 0.6 collective-permute-done
  6.7 0.0 copy-start.5
  6.7 0.0 copy-start.6
  6.8 1.5 %subtract_multiply_fusion.1 = f32[512,128]{1,0:T(8,128)S(1)} fusion(f32[542,128]{1,0:T(8,128)S(1)} %maximum_convert_fusion, f32[512]{0:T(512)} %param.13, f32[128]{0:T(128)S(1)} %get-tuple-element.43, f32[128]{0:T(128)S(1)} %get-tuple-element.44, f32[128]{0:T(128)S(1)} %get-tuple-element.45, f32[128]{0:T(128)S(1)} %get-tuple-element.46, ...), kind=kLoop, calls=%fused_computation.184 | loop fusion | flops 4128768 | bytes 8408576 | tf_op jit(solution)/shard_map/mul | solution.py:42
  8.3 0.0 copy-done
  8.3 0.0 copy-done.5
  8.3 0.0 copy-done.6
  8.3 0.0 copy-start.3
  8.3 0.0 copy-start.4
  8.3 0.8 multiply_reduce_fusion
  9.2 17.3 %all_to_all.20 = f32[8,1,1024]{2,1,0:T(1,128)S(1)} all-to-all(f32[8,1,1024]{2,1,0:T(1,128)S(1)} %broadcast_in_dim.6), channel_id=1, replica_groups=mesh['z'=16,'y'=8,'tp'=8] {'tp'}, dimensions={0} | all-to-all | bytes 65536 | tf_op jit(solution)/shard_map/all_to_all | solution.py:18
  26.6 0.0 copy-done.3
  26.6 0.0 copy-done.4
  26.6 2.2 %multiply_reduce_fusion.1 = (f32[128]{0:T(128)S(1)}, f32[128]{0:T(128)S(1)}, f32[128]{0:T(128)S(1)}, f32[128]{0:T(128)S(1)}, f32[128]{0:T(128)S(1)}, /*index=5*/...) fusion(f32[542,128]{1,0:T(8,128)S(1)} %maximum_convert_fusion, ...), kind=kLoop, calls=%fused_computation.148 | loop fusion | flops 6813440 | bytes 8684544 | tf_op jit(solution)/shard_map/reduce_sum | solution.py:72
  28.8 0.4 multiply_reduce_fusion.19
  29.2 0.1 stack.143
  29.3 0.7 broadcast_in_dim.7
  29.9 3.6 %all-to-all-start.2 = ((f32[8,32,128]{2,1,0:T(8,128)}), f32[8,32,128]{2,1,0:T(8,128)S(1)}, u32[]{:S(2)}, u32[]{:S(2)}) async-start(f32[8,32,128]{2,1,0:T(8,128)} %broadcast_in_dim.7), calls=%async_computation.2 | async-start | bytes 262144 | tf_op jit(solution)/shard_map/all_to_all | solution.py:18
  33.5 1.3 %fusion = bf16[2048,128]{0,1:T(8,128)(2,1)} fusion(bf16[512,2048]{1,0:T(8,128)(2,1)S(1)} %copy-done, f32[512,128]{1,0:T(8,128)S(1)} %subtract_multiply_fusion.1, f32[128]{0:T(128)S(1)} %copy-done.5), kind=kOutput, calls=%fused_computation.30 | convolution fusion | flops 269090816 | bytes 2884096 | tf_op jit(solution)/shard_map/dot_general | solution.py:54
  34.8 1.3 %copy.18 = bf16[2048,128]{1,0:T(8,128)(2,1)S(1)} copy(bf16[2048,128]{0,1:T(8,128)(2,1)} %fusion) | data formatting | bytes 1048576 | tf_op jit(solution)/shard_map/convert_element_type | solution.py:58
  36.1 0.0 copy-start.1
  36.1 0.0 copy-start.2
  36.1 0.8 copy.19
  37.0 5.6 %all-to-all-done.2 = f32[8,32,128]{2,1,0:T(8,128)S(1)} async-done(((f32[8,32,128]{2,1,0:T(8,128)}), f32[8,32,128]{2,1,0:T(8,128)S(1)}, u32[]{:S(2)}, u32[]{:S(2)}) %all-to-all-start.2) | async-done | bytes 131104 | tf_op jit(solution)/shard_map/all_to_all | solution.py:18
  42.6 3.5 %all-to-all-start.1 = ((bf16[8,256,128]{2,1,0:T(8,128)(2,1)}), bf16[8,256,128]{2,1,0:T(8,128)(2,1)S(1)}, u32[]{:S(2)}, u32[]{:S(2)}) async-start(bf16[8,256,128]{2,1,0:T(8,128)(2,1)} %bitcast.39), calls=%async_computation.1 | async-start | bytes 1048576 | tf_op jit(solution)/shard_map/all_to_all | solution.py:18
  46.1 16.0 %all-to-all-done.1 = bf16[8,256,128]{2,1,0:T(8,128)(2,1)S(1)} async-done(((bf16[8,256,128]{2,1,0:T(8,128)(2,1)}), bf16[8,256,128]{2,1,0:T(8,128)(2,1)S(1)}, u32[]{:S(2)}, u32[]{:S(2)}) %all-to-all-start.1) | async-done | bytes 524320 | tf_op jit(solution)/shard_map/all_to_all | solution.py:18
  62.1 0.1 reduce_sum.351
  62.2 0.7 pad_maximum_fusion.1
  62.9 15.6 %all-to-all-start.3 = ((bf16[16,48,128]{2,1,0:T(8,128)(2,1)}), bf16[16,48,128]{2,1,0:T(8,128)(2,1)S(1)}, u32[]{:S(2)}, u32[]{:S(2)}) async-start(bf16[16,48,128]{2,1,0:T(8,128)(2,1)} %pad_maximum_fusion.1), calls=%async_computation.3 | async-start | bytes 393216 | tf_op jit(solution)/shard_map/all_to_all | solution.py:18
  78.5 1.3 %collective-permute-start.1 = (f32[30,128]{1,0:T(8,128)S(1)}, f32[30,128]{1,0:T(8,128)S(1)}, u32[]{:S(2)}, u32[]{:S(2)}) collective-permute-start(f32[30,128]{1,0:T(8,128)S(1)} %slice.525), channel_id=1, source_target_pairs={{8,0},{16,8},{24,16},{32,24},{40,32},{48,40},{56,48},{64,56},{72,6... | collective-permute-start | bytes 46088 | tf_op jit(solution)/shard_map/ppermute | solution.py:14
  79.8 4.3 %collective-permute-done.1 = f32[30,128]{1,0:T(8,128)S(1)} collective-permute-done((f32[30,128]{1,0:T(8,128)S(1)}, f32[30,128]{1,0:T(8,128)S(1)}, u32[]{:S(2)}, u32[]{:S(2)}) %collective-permute-start.1) | collective-permute-done | bytes 15392 | tf_op jit(solution)/shard_map/ppermute | solution.py:14
  84.2 0.0 copy-done.1
  84.2 0.0 copy-done.2
  84.2 1.6 %fusion.5 = (bf16[512,128]{1,0:T(8,128)(2,1)}, f32[512,128]{1,0:T(8,128)S(1)}) fusion(bf16[512,128]{1,0:T(8,128)(2,1)S(1)} %copy-done.2, bf16[512,128]{1,0:T(8,128)(2,1)S(1)} %copy-done.1, f32[512,128]{1,0:T(8,128)S(1)} %get-tuple-element.39, f32[128]{0:T(128)S(1)} %get-tuple-element.43, f32[30,128]{1,0:T(8,128)S(1)} %collective-permute-done.1, ...), kind=kLoop, calls=%fused_computation.39 | loop fusion | flops 6619136 | bytes 948736 | tf_op jit(solution)/shard_map/convert_element_type | solution.py:76
  85.7 0.7 multiply_convert_fusion.1
  86.5 7.5 %all-to-all-done.3 = bf16[16,48,128]{2,1,0:T(8,128)(2,1)S(1)} async-done(((bf16[16,48,128]{2,1,0:T(8,128)(2,1)}), bf16[16,48,128]{2,1,0:T(8,128)(2,1)S(1)}, u32[]{:S(2)}, u32[]{:S(2)}) %all-to-all-start.3) | async-done | bytes 196640 | tf_op jit(solution)/shard_map/all_to_all | solution.py:18
  94.0 0.5 slice_bitcast_fusion
  94.5 0.6 slice.586
  95.1 0.6 slice.584
  (13 shorter events, 0.2 us)
Async XLA Ops:
  0.6 7.7 %copy-start = (bf16[512,2048]{1,0:T(8,128)(2,1)S(1)}, bf16[512,2048]{1,0:T(8,128)(2,1)}, u32[]{:S(2)}) copy-start(bf16[512,2048]{1,0:T(8,128)(2,1)} %param.15) | copy-start | bytes 6291460
  1.9 4.8 %collective-permute-start = (bf16[30,128]{1,0:T(8,128)(2,1)S(1)}, bf16[30,128]{1,0:T(8,128)(2,1)S(1)}, u32[]{:S(2)}, u32[]{:S(2)}) collective-permute-start(bf16[30,128]{1,0:T(8,128)(2,1)S(1)} %slice.461), channel_id=1, source_target_pairs={{0,8},{8,16},{16,24},{24,32},{32,40},{40,48},{48,56},{56,64},{64,7... | collective-permute-start | bytes 23048 | tf_op jit(solution)/shard_map/ppermute | solution.py:14
  6.7 1.6 %copy-start.5 = (f32[128]{0:T(128)S(1)}, f32[128]{0:T(128)}, u32[]{:S(2)}) copy-start(f32[128]{0:T(128)} %param.11) | copy-start | bytes 1540
  6.7 1.6 %copy-start.6 = (bf16[2048,128]{1,0:T(8,128)(2,1)S(1)}, bf16[2048,128]{1,0:T(8,128)(2,1)}, u32[]{:S(2)}) copy-start(bf16[2048,128]{1,0:T(8,128)(2,1)} %param.12) | copy-start | bytes 1572868
  8.3 18.3 %copy-start.3 = (f32[512]{0:T(512)S(1)}, f32[512]{0:T(512)}, u32[]{:S(2)}) copy-start(f32[512]{0:T(512)} %param.13) | copy-start | bytes 6148
  8.3 18.3 %copy-start.4 = (f32[512]{0:T(512)S(1)}, f32[512]{0:T(512)}, u32[]{:S(2)}) copy-start(f32[512]{0:T(512)} %param.14) | copy-start | bytes 6148
  29.9 12.6 %all-to-all-start.2 = ((f32[8,32,128]{2,1,0:T(8,128)}), f32[8,32,128]{2,1,0:T(8,128)S(1)}, u32[]{:S(2)}, u32[]{:S(2)}) async-start(f32[8,32,128]{2,1,0:T(8,128)} %broadcast_in_dim.7), calls=%async_computation.2 | async-start | bytes 262144 | tf_op jit(solution)/shard_map/all_to_all | solution.py:18
  36.1 48.0 %copy-start.1 = (bf16[512,128]{1,0:T(8,128)(2,1)S(1)}, bf16[512,128]{1,0:T(8,128)(2,1)}, u32[]{:S(2)}) copy-start(bf16[512,128]{1,0:T(8,128)(2,1)} %param.9) | copy-start | bytes 393220
  36.1 48.0 %copy-start.2 = (bf16[512,128]{1,0:T(8,128)(2,1)S(1)}, bf16[512,128]{1,0:T(8,128)(2,1)}, u32[]{:S(2)}) copy-start(bf16[512,128]{1,0:T(8,128)(2,1)} %param.8) | copy-start | bytes 393220
  42.6 19.5 %all-to-all-start.1 = ((bf16[8,256,128]{2,1,0:T(8,128)(2,1)}), bf16[8,256,128]{2,1,0:T(8,128)(2,1)S(1)}, u32[]{:S(2)}, u32[]{:S(2)}) async-start(bf16[8,256,128]{2,1,0:T(8,128)(2,1)} %bitcast.39), calls=%async_computation.1 | async-start | bytes 1048576 | tf_op jit(solution)/shard_map/all_to_all | solution.py:18
  62.9 31.1 %all-to-all-start.3 = ((bf16[16,48,128]{2,1,0:T(8,128)(2,1)}), bf16[16,48,128]{2,1,0:T(8,128)(2,1)S(1)}, u32[]{:S(2)}, u32[]{:S(2)}) async-start(bf16[16,48,128]{2,1,0:T(8,128)(2,1)} %pad_maximum_fusion.1), calls=%async_computation.3 | async-start | bytes 393216 | tf_op jit(solution)/shard_map/all_to_all | solution.py:18
  78.5 5.6 %collective-permute-start.1 = (f32[30,128]{1,0:T(8,128)S(1)}, f32[30,128]{1,0:T(8,128)S(1)}, u32[]{:S(2)}, u32[]{:S(2)}) collective-permute-start(f32[30,128]{1,0:T(8,128)S(1)} %slice.525), channel_id=1, source_target_pairs={{8,0},{16,8},{24,16},{32,24},{40,32},{48,40},{56,48},{64,56},{72,6... | collective-permute-start | bytes 46088 | tf_op jit(solution)/shard_map/ppermute | solution.py:14

commit v2 on v1

--- a/solution.py
+++ b/solution.py
@@ -33,7 +33,11 @@
     val_float = glu_value.astype(f32)
     gate_sig = jax.nn.sigmoid(glu_gate.astype(f32))
     gated = (val_float * gate_sig).astype(bf16)
-    before = passed_along(gated[tok_rows - reach_back :], SP, 1)
+    last_rows = lax.optimization_barrier(
+        (glu_value[tok_rows - reach_back :], glu_gate[tok_rows - reach_back :])
+    )
+    last_gated = last_rows[0].astype(f32) * jax.nn.sigmoid(last_rows[1].astype(f32))
+    before = passed_along(last_gated.astype(bf16), SP, 1)
     padded = jnp.concatenate([before, gated], axis=0).astype(f32)
     taps_float = conv_taps.astype(f32)
     conv = jnp.zeros(gated.shape, f32)
@@ -57,7 +61,6 @@
     own_rows = weight_part.shape[0] // (n_z * n_y)
     weight_part = weight_part.astype(bf16).reshape(n_z, n_y, own_rows, chans)
     weight_part = weight_part.transpose(1, 0, 2, 3).reshape(n_y, n_z * own_rows, chans)
-    weight_part = exchange(weight_part, "y").astype(f32).sum(axis=0)
 
     conv_grad = norm_scale[:, None] * (
         scaled_grad - mean_plain[:, None] - centered * mean_cross[:, None]
@@ -70,15 +73,19 @@
         begin = reach_back - offset
         gated_grad = gated_grad + taps_float[offset] * grad_padded[begin : begin + tok_rows]
         tap_list.append(jnp.sum(conv_grad * padded[offset : offset + tok_rows], axis=0))
-    small = jnp.stack([*tap_list, gain_local], axis=0)
-    small = to_all(small, "y").sum(axis=0).astype(bf16)
+    small = jnp.stack([*tap_list, gain_local], axis=0).astype(bf16)
+    n_big = n_z * own_rows
+    both = jnp.concatenate(
+        [weight_part, jnp.broadcast_to(small, (n_y, *small.shape))], axis=1
+    )
+    both = exchange(both, "y").astype(f32).sum(axis=0).astype(bf16)
     value_grad = (gated_grad * gate_sig).astype(bf16)
     gate_grad = (gated_grad * val_float * gate_sig * (1.0 - gate_sig)).astype(bf16)
 
     last = jnp.concatenate(
         [
-            weight_part.astype(bf16).reshape(n_z, own_rows, chans),
-            jnp.broadcast_to(small, (n_z, *small.shape)),
+            both[:n_big].reshape(n_z, own_rows, chans),
+            jnp.broadcast_to(both[n_big:], (n_z, *small.shape)),
         ],
         axis=1,
     )

time: 96.3 us -> 89.3 us (0.927)
  the two profiles are of different devices: /device:TPU:2 before, /device:TPU:4 now
where the time goes in v2:
time: 89.3 us; the launch traced here: 88.7 us
  starting transfers between devices  33.6 us (38%)
  blocking collectives  22 us (25%)
  waiting for transfers between devices  11.9 us (13%)
  other arithmetic  10.5 us (12%)
  local copies, waits for them, and re-layouts  7.07 us (8%)
  matrix products  2.42 us (3%)
  between operations  1.19 us (1%)
    all_to_all x2, starting transfers between devices, exchange(): return lax.all_to_all(value, axis, split_axis=0, concat_axis=0, tiled=True)  28.9 us
    all_to_all x1, blocking collectives, exchange(): return lax.all_to_all(value, axis, split_axis=0, concat_axis=0, tiled=True)  22 us
    all_to_all x2, waiting for transfers between devices, exchange(): return lax.all_to_all(value, axis, split_axis=0, concat_axis=0, tiled=True)  7.59 us
    ppermute x2, starting transfers between devices, passed_along(): return lax.ppermute(value, axis, pairs)  4.77 us
    ppermute x2, waiting for transfers between devices, passed_along(): return lax.ppermute(value, axis, pairs)  4.34 us
    reduce_sum x2, other arithmetic, per_device(): jnp.sum(conv_grad * padded[offset:offset + tok_rows], axis=0)  3.97 us
  transfers between devices with their start and end apart: 4, of which 2 were waited for; matrix products, arithmetic and copies ran while one was open for 8% of the time, Pallas kernels for 0%

profile of v2, /device:TPU:4, one launch (start us, length us, event | category | flops | bytes accessed | tf_op | source)
XLA Modules:
  0.0 88.7 jit_solution(17424940233775855918)
XLA Ops:
  0.6 0.0 copy-start
  0.6 0.9 slice.371
  1.5 0.7 slice.372
  2.2 3.5 %collective-permute-start = (bf16[30,128]{1,0:T(8,128)(2,1)S(1)}, bf16[30,128]{1,0:T(8,128)(2,1)S(1)}, u32[]{:S(2)}, u32[]{:S(2)}) collective-permute-start(bf16[30,128]{1,0:T(8,128)(2,1)S(1)} %multiply_convert_fusion.3), channel_id=1, source_target_pairs={{0,8},{8,16},{16,24},{24,32},{32,40},{40,48},{48,56},{56,64},{64,7... | collective-permute-start | bytes 23048 | tf_op jit(solution)/shard_map/ppermute | solution.py:14
  5.7 1.0 %fusion.2 = bf16[512,128]{1,0:T(8,128)(2,1)S(1)} fusion(bf16[512,128]{1,0:T(8,128)(2,1)} %param.8, bf16[512,128]{1,0:T(8,128)(2,1)} %param.9), kind=kLoop, calls=%fused_computation.37 | loop fusion | flops 458752 | bytes 393216 | tf_op jit(solution)/shard_map/convert_element_type | solution.py:35
  6.8 0.7 convert_element_type.45
  7.5 0.0 copy-start.5
  7.5 0.0 copy-start.7
  7.5 0.0 copy-start.9
  7.5 0.0 copy-start.11
  7.6 0.0 collective-permute-done
  7.6 0.4 copy-done.5
  8.0 0.0 copy-done.7
  8.0 0.0 copy-done.9
  8.0 0.1 copy-done.11
  8.1 0.0 copy-done.15
  8.1 0.0 copy-done.21
  8.2 0.0 copy-start.37
  8.2 1.5 %subtract_multiply_fusion.1 = f32[512,128]{1,0:T(8,128)S(1)} fusion(f32[542,128]{1,0:T(8,128)S(1)} %maximum_convert_fusion, f32[512]{0:T(512)} %param.13, f32[128]{0:T(128)S(1)} %get-tuple-element.47, f32[128]{0:T(128)S(1)} %get-tuple-element.48, f32[128]{0:T(128)S(1)} %get-tuple-element.49, f32[128]{0:T(128)S(1)} %get-tuple-element.50, ...), kind=kLoop, calls=%fused_computation.185 | loop fusion | flops 4128768 | bytes 8408576 | tf_op jit(solution)/shard_map/mul | solution.py:46
  9.7 1.2 %multiply_reduce_fusion = (bf16[128]{0:T(256)(128)(2,1)}, f32[512]{0:T(512)S(1)}, f32[512]{0:T(512)S(1)}, f32[512,128]{1,0:T(8,128)S(1)}) fusion(f32[512,128]{1,0:T(8,128)S(1)} %subtract_multiply_fusion.1, f32[128]{0:T(128)S(1)} %copy-done.23, bf16[512,2048]{1,0:T(8,128)(2,1)S(1)} %copy-done, bf16[2048,128]{1,0:T(8,128)(2,1)S(1)} %copy-done.37), kind=kOutput, calls=%fused_computation.148 | convolution fusion | flops 269417344 | bytes 3150592 | tf_op jit(solution)/shard_map/dot_general | solution.py:50
  11.0 0.6 broadcast_in_dim.6
  11.6 14.2 %all-to-all-start = ((f32[8,1,1024]{2,1,0:T(1,128)}), f32[8,1,1024]{2,1,0:T(1,128)S(1)}, u32[]{:S(2)}, u32[]{:S(2)}) async-start(f32[8,1,1024]{2,1,0:T(1,128)} %broadcast_in_dim.6), calls=%async_computation | async-start | bytes 65536 | tf_op jit(solution)/shard_map/all_to_all | solution.py:18
  25.8 1.2 %fusion = bf16[2048,128]{0,1:T(8,128)(2,1)S(1)} fusion(bf16[512,2048]{1,0:T(8,128)(2,1)S(1)} %copy-done, f32[512,128]{1,0:T(8,128)S(1)} %subtract_multiply_fusion.1, f32[128]{0:T(128)} %param.11), kind=kOutput, calls=%fused_computation.30 | convolution fusion | flops 269090816 | bytes 2884096 | tf_op jit(solution)/shard_map/dot_general | solution.py:58
  27.0 1.0 %copy.18 = bf16[2048,128]{1,0:T(8,128)(2,1)} copy(bf16[2048,128]{0,1:T(8,128)(2,1)S(1)} %fusion) | data formatting | bytes 1048576 | tf_op jit(solution)/shard_map/convert_element_type | solution.py:62
  28.0 1.1 %copy.19 = bf16[8,16,16,128]{3,2,1,0:T(8,128)(2,1)S(1)} copy(bf16[8,16,16,128]{3,2,0,1:T(8,128)(2,1)} %bitcast.179) | data formatting | bytes 1048576 | tf_op jit(solution)/shard_map/transpose | solution.py:63
  29.1 0.0 all-to-all-done
  29.2 3.6 %multiply_reduce_fusion.1 = (bf16[128]{0:T(256)(128)(2,1)S(1)}, bf16[128]{0:T(256)(128)(2,1)S(1)}, bf16[128]{0:T(256)(128)(2,1)S(1)}, bf16[128]{0:T(256)(128)(2,...) fusion(f32[542,128]{1,0:T(8,128)S(1)} %maximum_convert_fusion, ...), kind=kLoop, calls=%fused_computation.149 | loop fusion | flops 6813440 | bytes 8679936 | tf_op jit(solution)/shard_map/reduce_sum | solution.py:75
  32.9 0.0 copy-start.36
  32.9 0.4 multiply_reduce_fusion.19
  33.2 0.2 copy-done.24
  33.4 0.0 copy-done.25
  33.5 0.1 stack.176
  33.7 0.0 copy-start.2
  33.7 0.0 copy-start.6
  33.7 0.0 copy-start.8
  33.7 0.0 copy-start.10
  33.9 22.0 %all_to_all.15 = bf16[8,288,128]{2,1,0:T(8,128)(2,1)S(1)} all-to-all(bf16[8,288,128]{2,1,0:T(8,128)(2,1)S(1)} %pad_maximum_fusion), channel_id=1, replica_groups=mesh['z'=16,'y'=8,'tp'=8] {'y'}, dimensions={0} | all-to-all | bytes 1179648 | tf_op jit(solution)/shard_map/all_to_all | solution.py:18
  55.8 0.1 reduce_sum.374
  56.0 0.7 pad_maximum_fusion.2
  56.7 14.7 %all-to-all-start.2 = ((bf16[16,48,128]{2,1,0:T(8,128)(2,1)}), bf16[16,48,128]{2,1,0:T(8,128)(2,1)S(1)}, u32[]{:S(2)}, u32[]{:S(2)}) async-start(bf16[16,48,128]{2,1,0:T(8,128)(2,1)} %pad_maximum_fusion.2), calls=%async_computation.2 | async-start | bytes 393216 | tf_op jit(solution)/shard_map/all_to_all | solution.py:18
  71.3 1.3 %collective-permute-start.1 = (f32[30,128]{1,0:T(8,128)S(1)}, f32[30,128]{1,0:T(8,128)S(1)}, u32[]{:S(2)}, u32[]{:S(2)}) collective-permute-start(f32[30,128]{1,0:T(8,128)S(1)} %slice.536), channel_id=1, source_target_pairs={{8,0},{16,8},{24,16},{32,24},{40,32},{48,40},{56,48},{64,56},{72,6... | collective-permute-start | bytes 46088 | tf_op jit(solution)/shard_map/ppermute | solution.py:14
  72.6 4.3 %collective-permute-done.1 = f32[30,128]{1,0:T(8,128)S(1)} collective-permute-done((f32[30,128]{1,0:T(8,128)S(1)}, f32[30,128]{1,0:T(8,128)S(1)}, u32[]{:S(2)}, u32[]{:S(2)}) %collective-permute-start.1) | collective-permute-done | bytes 15392 | tf_op jit(solution)/shard_map/ppermute | solution.py:14
  77.1 1.6 %fusion.5 = (bf16[512,128]{1,0:T(8,128)(2,1)}, f32[512,128]{1,0:T(8,128)S(1)}) fusion(bf16[512,128]{1,0:T(8,128)(2,1)S(1)} %copy-done.2, bf16[512,128]{1,0:T(8,128)(2,1)S(1)} %copy-done.1, f32[512,128]{1,0:T(8,128)S(1)} %get-tuple-element.43, f32[128]{0:T(128)S(1)} %get-tuple-element.47, f32[30,128]{1,0:T(8,128)S(1)} %collective-permute-done.1, ...), kind=kLoop, calls=%fused_computation.40 | loop fusion | flops 6619136 | bytes 948736 | tf_op jit(solution)/shard_map/convert_element_type | solution.py:83
  78.7 0.7 multiply_convert_fusion.1
  79.4 7.6 %all-to-all-done.2 = bf16[16,48,128]{2,1,0:T(8,128)(2,1)S(1)} async-done(((bf16[16,48,128]{2,1,0:T(8,128)(2,1)}), bf16[16,48,128]{2,1,0:T(8,128)(2,1)S(1)}, u32[]{:S(2)}, u32[]{:S(2)}) %all-to-all-start.2) | async-done | bytes 196640 | tf_op jit(solution)/shard_map/all_to_all | solution.py:18
  87.0 0.5 slice_bitcast_fusion
  87.5 0.6 slice.599
  88.1 0.6 slice.597
  (72 shorter events, 0.4 us)
Async XLA Ops:
  0.6 9.1 %copy-start = (bf16[512,2048]{1,0:T(8,128)(2,1)S(1)}, bf16[512,2048]{1,0:T(8,128)(2,1)}, u32[]{:S(2)}) copy-start(bf16[512,2048]{1,0:T(8,128)(2,1)} %param.15) | copy-start | bytes 6291460
  2.2 5.4 %collective-permute-start = (bf16[30,128]{1,0:T(8,128)(2,1)S(1)}, bf16[30,128]{1,0:T(8,128)(2,1)S(1)}, u32[]{:S(2)}, u32[]{:S(2)}) collective-permute-start(bf16[30,128]{1,0:T(8,128)(2,1)S(1)} %multiply_convert_fusion.3), channel_id=1, source_target_pairs={{0,8},{8,16},{16,24},{24,32},{32,40},{40,48},{48,56},{56,64},{64,7... | collective-permute-start | bytes 23048 | tf_op jit(solution)/shard_map/ppermute | solution.py:14
  7.5 0.5 copy-start.5
  7.5 0.5 copy-start.7
  7.5 0.5 copy-start.9
  7.5 0.6 copy-start.11
  7.5 0.6 copy-start.13
  7.5 0.6 copy-start.15
  7.6 0.6 copy-start.17
  7.6 0.6 copy-start.19
  7.6 0.6 copy-start.21
  8.2 1.6 %copy-start.23 = (f32[128]{0:T(128)S(1)}, f32[128]{0:T(128)}, u32[]{:S(2)}) copy-start(f32[128]{0:T(128)} %param.11) | copy-start | bytes 1540
  8.2 1.6 %copy-start.37 = (bf16[2048,128]{1,0:T(8,128)(2,1)S(1)}, bf16[2048,128]{1,0:T(8,128)(2,1)}, u32[]{:S(2)}) copy-start(bf16[2048,128]{1,0:T(8,128)(2,1)} %param.12) | copy-start | bytes 1572868
  11.6 17.5 %all-to-all-start = ((f32[8,1,1024]{2,1,0:T(1,128)}), f32[8,1,1024]{2,1,0:T(1,128)S(1)}, u32[]{:S(2)}, u32[]{:S(2)}) async-start(f32[8,1,1024]{2,1,0:T(1,128)} %broadcast_in_dim.6), calls=%async_computation | async-start | bytes 65536 | tf_op jit(solution)/shard_map/all_to_all | solution.py:18
  25.8 3.3 %copy-start.3 = (f32[512]{0:T(512)S(1)}, f32[512]{0:T(512)}, u32[]{:S(2)}) copy-start(f32[512]{0:T(512)} %param.13) | copy-start | bytes 6148
  25.8 3.3 %copy-start.4 = (f32[512]{0:T(512)S(1)}, f32[512]{0:T(512)}, u32[]{:S(2)}) copy-start(f32[512]{0:T(512)} %param.14) | copy-start | bytes 6148
  32.8 0.7 copy-start.24
  32.8 0.7 copy-start.25
  32.8 0.7 copy-start.26
  32.8 0.7 copy-start.27
  32.8 0.7 copy-start.28
  32.8 0.7 copy-start.29
  32.8 0.7 copy-start.30
  32.8 0.7 copy-start.31
  32.8 0.7 copy-start.32
  32.8 0.7 copy-start.33
  32.8 0.7 copy-start.34
  32.8 0.7 copy-start.35
  32.9 0.7 copy-start.36
  33.7 43.3 %copy-start.1 = (bf16[512,128]{1,0:T(8,128)(2,1)S(1)}, bf16[512,128]{1,0:T(8,128)(2,1)}, u32[]{:S(2)}) copy-start(bf16[512,128]{1,0:T(8,128)(2,1)} %param.9) | copy-start | bytes 393220
  33.7 43.3 %copy-start.2 = (bf16[512,128]{1,0:T(8,128)(2,1)S(1)}, bf16[512,128]{1,0:T(8,128)(2,1)}, u32[]{:S(2)}) copy-start(bf16[512,128]{1,0:T(8,128)(2,1)} %param.8) | copy-start | bytes 393220
  33.7 43.3 %copy-start.6 = (f32[128]{0:T(128)S(1)}, f32[128]{0:T(128)}, u32[]{:S(2)}) copy-start(f32[128]{0:T(128)} %copy-done.5) | copy-start | bytes 1540
  33.7 43.3 %copy-start.8 = (f32[128]{0:T(128)S(1)}, f32[128]{0:T(128)}, u32[]{:S(2)}) copy-start(f32[128]{0:T(128)} %copy-done.7) | copy-start | bytes 1540
  33.7 43.3 %copy-start.10 = (f32[128]{0:T(128)S(1)}, f32[128]{0:T(128)}, u32[]{:S(2)}) copy-start(f32[128]{0:T(128)} %copy-done.9) | copy-start | bytes 1540
  33.7 43.3 %copy-start.12 = (f32[128]{0:T(128)S(1)}, f32[128]{0:T(128)}, u32[]{:S(2)}) copy-start(f32[128]{0:T(128)} %copy-done.11) | copy-start | bytes 1540
  33.7 43.3 %copy-start.14 = (f32[128]{0:T(128)S(1)}, f32[128]{0:T(128)}, u32[]{:S(2)}) copy-start(f32[128]{0:T(128)} %copy-done.13) | copy-start | bytes 1540
  33.7 43.3 %copy-start.16 = (f32[128]{0:T(128)S(1)}, f32[128]{0:T(128)}, u32[]{:S(2)}) copy-start(f32[128]{0:T(128)} %copy-done.15) | copy-start | bytes 1540
  33.8 43.3 %copy-start.18 = (f32[128]{0:T(128)S(1)}, f32[128]{0:T(128)}, u32[]{:S(2)}) copy-start(f32[128]{0:T(128)} %copy-done.17) | copy-start | bytes 1540
  33.8 43.3 %copy-start.20 = (f32[128]{0:T(128)S(1)}, f32[128]{0:T(128)}, u32[]{:S(2)}) copy-start(f32[128]{0:T(128)} %copy-done.19) | copy-start | bytes 1540
  33.8 43.3 %copy-start.22 = (f32[128]{0:T(128)S(1)}, f32[128]{0:T(128)}, u32[]{:S(2)}) copy-start(f32[128]{0:T(128)} %copy-done.21) | copy-start | bytes 1540
  56.7 30.3 %all-to-all-start.2 = ((bf16[16,48,128]{2,1,0:T(8,128)(2,1)}), bf16[16,48,128]{2,1,0:T(8,128)(2,1)S(1)}, u32[]{:S(2)}, u32[]{:S(2)}) async-start(bf16[16,48,128]{2,1,0:T(8,128)(2,1)} %pad_maximum_fusion.2), calls=%async_computation.2 | async-start | bytes 393216 | tf_op jit(solution)/shard_map/all_to_all | solution.py:18
  71.3 5.6 %collective-permute-start.1 = (f32[30,128]{1,0:T(8,128)S(1)}, f32[30,128]{1,0:T(8,128)S(1)}, u32[]{:S(2)}, u32[]{:S(2)}) collective-permute-start(f32[30,128]{1,0:T(8,128)S(1)} %slice.536), channel_id=1, source_target_pairs={{8,0},{16,8},{24,16},{32,24},{40,32},{48,40},{56,48},{64,56},{72,6... | collective-permute-start | bytes 46088 | tf_op jit(solution)/shard_map/ppermute | solution.py:14

commit v3 on v1

v3 whole, which is shorter than its diff:
```python
import functools

import jax
import jax.numpy as jnp
from jax import lax
from jax.experimental import pallas as pl
from jax.experimental.pallas import tpu as pltpu
from jax.sharding import Mesh
from jax.sharding import PartitionSpec as P

SP = ("z", "y")
HALO = 32
BLOCK = 64
LANES = 128
F32, BF16 = jnp.float32, jnp.bfloat16
VMEM = pl.BlockSpec(memory_space=pltpu.VMEM)
HBM = pl.BlockSpec(memory_space=pltpu.HBM)


def column(row):
    return jnp.transpose(jnp.broadcast_to(row, (LANES, LANES)))


def row_sums(block):
    return jnp.sum(jnp.transpose(block), axis=0, keepdims=True)


def weighted(taps_ref, source_ref, first, rows, step):
    total = None
    for k in range(taps_ref.shape[0] - 1):
        begin = first + step * k
        term = taps_ref[k : k + 1, :] * source_ref[begin : begin + rows, :]
        total = term if total is None else total + term
    return total


def silu_parts(conv, mean, scale, gain, act_grad):
    centered = (conv - mean) * scale
    normed = centered * gain
    sig = jax.nn.sigmoid(normed)
    normed_grad = act_grad * sig * (1.0 + normed * (1.0 - sig))
    return centered, (normed * sig).astype(BF16), normed_grad, normed_grad * gain


def tail_kernel(value_ref, gate_ref, out_ref, value_rows, gate_rows, sems):
    first = value_ref.shape[0] - HALO
    copies = [
        pltpu.make_async_copy(ref.at[pl.ds(first, HALO)], rows, sems.at[i])
        for i, (ref, rows) in enumerate(((value_ref, value_rows), (gate_ref, gate_rows)))
    ]
    for c in copies:
        c.start()
    for c in copies:
        c.wait()
    sig = jax.nn.sigmoid(gate_rows[...].astype(F32))
    out_ref[...] = (value_rows[...].astype(F32) * sig).astype(BF16)


def main_kernel(
    value_in, gate_in, taps_in, gain_in, mean_in, scale_in, weight_in, out_grad_in,
    taps, gain_ref, mean_ref, scale_ref, out_grad_ref,
    gated_ref, centered_ref, scaled_ref, activated_ref, conv_first, act_first, gain_sum, sums_ref,
    value_ref, gate_ref, padded, taps_raw, weight_ref, conv_ref, sems,
):
    rows, taps_n = value_ref.shape[0], taps_in.shape[0]
    moved = (
        (value_in, value_ref), (gate_in, gate_ref), (taps_in, taps_raw), (gain_in, gain_ref),
        (mean_in, mean_ref), (scale_in, scale_ref), (weight_in, weight_ref),
        (out_grad_in, out_grad_ref),
    )
    copies = [pltpu.make_async_copy(src, dst, sems.at[i]) for i, (src, dst) in enumerate(moved)]
    for c in copies:
        c.start()
    for c in copies[:3]:
        c.wait()
    taps[0:taps_n, :] = taps_raw[...].astype(F32)
    gated = (value_ref[...].astype(F32) * jax.nn.sigmoid(gate_ref[...].astype(F32))).astype(BF16)
    gated_ref[...] = gated
    padded[0:HALO, :] = jnp.zeros((HALO, LANES), F32)
    padded[HALO : HALO + rows, :] = gated.astype(F32)
    for r in range(0, rows, BLOCK):
        conv_ref[r : r + BLOCK, :] = weighted(taps, padded, 2 + r, BLOCK, 1)
    for c in copies[3:]:
        c.wait()
    conv_first[...] = conv_ref[0:HALO, :]
    gain = gain_ref[...]
    gain_total = jnp.zeros((8, LANES), F32)
    n_b = rows // LANES
    for b in range(n_b):
        at = b * LANES
        mean, scale = column(mean_ref[b : b + 1, :]), column(scale_ref[b : b + 1, :])
        act_grad = jnp.dot(
            out_grad_ref[at : at + LANES, :], weight_ref[...], preferred_element_type=F32
        )
        if b == 0:
            act_first[...] = act_grad[:HALO]
        plain, cross = [], []
        for h in range(0, LANES, BLOCK):
            r = at + h
            centered, activated, normed_grad, scaled = silu_parts(
                conv_ref[r : r + BLOCK, :], mean[h : h + BLOCK], scale[h : h + BLOCK], gain,
                act_grad[h : h + BLOCK],
            )
            centered_ref[r : r + BLOCK, :] = centered
            scaled_ref[r : r + BLOCK, :] = scaled
            activated_ref[r : r + BLOCK, :] = activated
            for_gain = normed_grad * centered
            if r == 0:
                for_gain = for_gain[HALO:]
            gain_total += jnp.sum(for_gain.reshape(-1, 8, LANES), axis=0)
            plain.append(scaled)
            cross.append(scaled * centered)
        sums_ref[b : b + 1, :] = row_sums(jnp.concatenate(plain, axis=0))
        sums_ref[n_b + b : n_b + b + 1, :] = row_sums(jnp.concatenate(cross, axis=0))
    gain_sum[...] = gain_total


def first_kernel(
    before_ref, conv_first, act_first, taps, gain_ref, mean_ref, scale_ref, gain_sum, sums_ref,
    centered_ref, scaled_ref, activated_ref, gain_out, sums_out,
    padded,
):
    padded[0:HALO, :] = before_ref[...].astype(F32)
    padded[HALO : 2 * HALO, :] = jnp.zeros((HALO, LANES), F32)
    conv = conv_first[...] + weighted(taps, padded, 2, HALO, 1)
    mean, scale = column(mean_ref[0:1, :])[:HALO], column(scale_ref[0:1, :])[:HALO]
    centered, activated, normed_grad, scaled = silu_parts(
        conv, mean, scale, gain_ref[...], act_first[...]
    )
    centered_ref[...] = centered
    scaled_ref[...] = scaled
    activated_ref[...] = activated
    gain_out[...] = gain_sum[...] + jnp.sum((normed_grad * centered).reshape(-1, 8, LANES), axis=0)
    filler = jnp.zeros((LANES - HALO, LANES), F32)
    plain = row_sums(jnp.concatenate([scaled, filler], axis=0))
    cross = row_sums(jnp.concatenate([scaled * centered, filler], axis=0))
    tile = sums_ref[...]
    n_b = tile.shape[0] // 2
    at_row = lax.broadcasted_iota(jnp.int32, tile.shape, 0)
    mine = lax.broadcasted_iota(jnp.int32, tile.shape, 1) < HALO
    tile = jnp.where((at_row == 0) & mine, plain, tile)
    tile = jnp.where((at_row == n_b) & mine, cross, tile)
    for j in range(sums_out.shape[0]):
        sums_out[j] = tile


def weight_kernel(out_grad_ref, activated_ref, activated_first, out_ref, *, n_z, n_y):
    activated = jnp.concatenate([activated_first[...], activated_ref[HALO:, :]], axis=0)
    part = lax.dot_general(
        out_grad_ref[...], activated, (((0,), (0,)), ((), ())), preferred_element_type=F32
    ).astype(BF16)
    own = part.shape[0] // (n_z * n_y)
    for z in range(n_z):
        for y in range(n_y):
            at = (z * n_y + y) * own
            out_ref[y, z * own : (z + 1) * own, :] = part[at : at + own]


def pack_kernel(
    all_sums, centered_ref, scaled_ref, centered_first, scaled_first, gated_ref, before_ref,
    scale_ref, part_ref, gain_sum,
    out_ref, conv_grad_ref, first_rows, padded,
    *, channels, taps_n,
):
    rows = gated_ref.shape[0]
    tile = all_sums[0]
    for j in range(1, all_sums.shape[0]):
        tile = tile + all_sums[j]
    tile = tile * (1.0 / channels)
    n_b = rows // LANES
    padded[0:HALO, :] = before_ref[...].astype(F32)
    padded[HALO : HALO + rows, :] = gated_ref[...].astype(F32)
    for b in range(n_b):
        at = b * LANES
        plain, cross = column(tile[b : b + 1]), column(tile[n_b + b : n_b + b + 1])
        scale = column(scale_ref[b : b + 1, :])
        centered, scaled = centered_ref[at : at + LANES, :], scaled_ref[at : at + LANES, :]
        if b == 0:
            centered = jnp.concatenate([centered_first[...], centered[HALO:]], axis=0)
            scaled = jnp.concatenate([scaled_first[...], scaled[HALO:]], axis=0)
        conv_grad_ref[at : at + LANES, :] = scale * (scaled - plain - centered * cross)
    first_rows[...] = conv_grad_ref[0:HALO, :]
    small = []
    for k0 in range(0, taps_n, 8):
        ks = range(k0, min(k0 + 8, taps_n))
        totals = {k: jnp.zeros((8, LANES), F32) for k in ks}
        for r in range(0, rows, 8):
            grad = conv_grad_ref[r : r + 8, :]
            for k in ks:
                totals[k] = totals[k] + grad * padded[2 + k + r : 10 + k + r, :]
        small += [jnp.sum(totals[k], axis=0, keepdims=True) for k in ks]
    small.append(jnp.sum(gain_sum[...], axis=0, keepdims=True))
    small = jnp.concatenate(small, axis=0).astype(BF16)
    big = part_ref.shape[1]
    for y in range(out_ref.shape[0]):
        out_ref[y, 0:big, :] = part_ref[y]
        out_ref[y, big : big + taps_n + 1, :] = small


def middle_kernel(in_ref, out_ref, *, own):
    total = in_ref[0].astype(F32)
    for y in range(1, in_ref.shape[0]):
        total = total + in_ref[y].astype(F32)
    total = total.astype(BF16)
    n_z = out_ref.shape[0]
    small = total[n_z * own :]
    for z in range(n_z):
        out_ref[z, 0:own, :] = total[z * own : (z + 1) * own]
        out_ref[z, own:, :] = small


def last_kernel(in_ref, weight_ref, taps_ref, gain_ref):
    total = in_ref[0].astype(F32)
    for z in range(1, in_ref.shape[0]):
        total = total + in_ref[z].astype(F32)
    own, taps_n = weight_ref.shape[0], taps_ref.shape[0]
    weight_ref[...] = total[0:own]
    taps_ref[...] = total[own : own + taps_n]
    gain_ref[...] = total[own + taps_n : own + taps_n + 1]


def glu_kernel(
    value_in, gate_in, conv_grad_ref, after_ref, taps, value_grad, gate_grad,
    value_ref, gate_ref, padded, sems,
):
    rows, taps_n = value_ref.shape[0], taps.shape[0] - 1
    moved = ((value_in, value_ref), (gate_in, gate_ref))
    copies = [pltpu.make_async_copy(src, dst, sems.at[i]) for i, (src, dst) in enumerate(moved)]
    for c in copies:
        c.start()
    padded[0:rows, :] = conv_grad_ref[...]
    padded[rows : rows + HALO, :] = after_ref[...]
    for c in copies:
        c.wait()
    for r in range(0, rows, BLOCK):
        gated_grad = weighted(taps, padded, r + taps_n - 1, BLOCK, -1)
        sig = jax.nn.sigmoid(gate_ref[r : r + BLOCK, :].astype(F32))
        value = value_ref[r : r + BLOCK, :].astype(F32)
        value_grad[r : r + BLOCK, :] = (gated_grad * sig).astype(BF16)
        gate_grad[r : r + BLOCK, :] = (gated_grad * value * sig * (1.0 - sig)).astype(BF16)


def passed_along(value, axis, by):
    length = lax.axis_size(axis)
    pairs = [(i, i + by) for i in range(length) if 0 <= i + by < length]
    return lax.ppermute(value, axis, pairs)


def exchange(value, axis):
    return lax.all_to_all(value, axis, split_axis=0, concat_axis=0, tiled=True)


def call(kernel, outs, in_specs, scratch=(), flops=0, final=False):
    run = pl.pallas_call(
        kernel,
        out_shape=[jax.ShapeDtypeStruct(*o) if final else pltpu.VMEM(*o) for o in outs],
        in_specs=in_specs,
        out_specs=[VMEM] * len(outs),
        scratch_shapes=list(scratch),
        cost_estimate=pl.CostEstimate(flops=flops, bytes_accessed=0, transcendentals=0),
        compiler_params=pltpu.CompilerParams(vmem_limit_bytes=16 << 20),
    )

    def with_operands(*operands):
        return run(
            *(
                pltpu.with_memory_space_constraint(x, spec.memory_space)
                for x, spec in zip(operands, in_specs)
            )
        )

    return with_operands


def per_device(
    glu_value, glu_gate, conv_taps, norm_gain, out_weight, norm_mean, norm_scale, out_grad
):
    rows, chans = glu_value.shape
    taps_n = conv_taps.shape[0]
    wide = out_grad.shape[1]
    n_z, n_y, n_tp = lax.axis_size("z"), lax.axis_size("y"), lax.axis_size("tp")
    own = wide // (n_z * n_y)
    n_b = rows // LANES
    gain = norm_gain.reshape(1, chans)
    mean, scale = norm_mean.reshape(n_b, LANES), norm_scale.reshape(n_b, LANES)
    full, few = (rows, chans), (HALO, chans)

    (tail,) = call(
        tail_kernel, [(few, BF16)], [HBM, HBM],
        [pltpu.VMEM(few, BF16), pltpu.VMEM(few, BF16), pltpu.SemaphoreType.DMA((2,))],
    )(glu_value, glu_gate)
    before = passed_along(tail, SP, 1)
    block = (n_b, LANES)
    (taps, gain, mean, scale, out_grad_here,
     gated, centered, scaled, activated, conv0, act0, gain_sum, sums) = call(
        main_kernel,
        [((taps_n + 1, chans), F32), ((1, chans), F32), (block, F32),
         (block, F32), ((rows, wide), BF16),
         (full, BF16), (full, F32), (full, F32), (full, BF16), (few, F32), (few, F32),
         ((8, chans), F32), ((2 * n_b, LANES), F32)],
        [HBM] * 8,
        [pltpu.VMEM(full, BF16), pltpu.VMEM(full, BF16),
         pltpu.VMEM((HALO + rows, chans), F32), pltpu.VMEM((taps_n, chans), BF16),
         pltpu.VMEM((wide, chans), BF16), pltpu.VMEM(full, F32), pltpu.SemaphoreType.DMA((8,))],
        flops=1 << 28,
    )(glu_value, glu_gate, conv_taps, gain, mean, scale, out_weight, out_grad)
    centered0, scaled0, activated0, gain_sum, sums = call(
        first_kernel,
        [(few, F32), (few, F32), (few, BF16), ((8, chans), F32), ((n_tp, 2 * n_b, LANES), F32)],
        [VMEM] * 9,
        [pltpu.VMEM((2 * HALO, chans), F32)],
        flops=1 << 24,
    )(before, conv0, act0, taps, gain, mean, scale, gain_sum, sums)
    sums = exchange(sums, "tp")
    (part,) = call(
        functools.partial(weight_kernel, n_z=n_z, n_y=n_y),
        [((n_y, n_z * own, chans), BF16)], [VMEM] * 3, flops=1 << 28,
    )(out_grad_here, activated, activated0)
    packed, conv_grad, first_rows = call(
        functools.partial(pack_kernel, channels=chans * n_tp, taps_n=taps_n),
        [((n_y, n_z * own + taps_n + 1, chans), BF16), (full, F32), (few, F32)],
        [VMEM] * 10,
        [pltpu.VMEM((HALO + rows, chans), F32)],
        flops=1 << 26,
    )(sums, centered, scaled, centered0, scaled0, gated, before, scale, part, gain_sum)
    packed = exchange(packed, "y")
    (packed,) = call(
        functools.partial(middle_kernel, own=own),
        [((n_z, own + taps_n + 1, chans), BF16)], [VMEM], flops=1 << 22,
    )(packed)
    packed = exchange(packed, "z")
    after = passed_along(first_rows, SP, -1)
    value_grad, gate_grad = call(
        glu_kernel, [(full, BF16), (full, BF16)], [HBM] * 2 + [VMEM] * 3,
        [pltpu.VMEM(full, BF16), pltpu.VMEM(full, BF16), pltpu.VMEM((rows + HALO, chans), F32),
         pltpu.SemaphoreType.DMA((2,))], flops=1 << 28, final=True,
    )(glu_value, glu_gate, conv_grad, after, taps)
    weight_grad, taps_grad, gain_grad = call(
        last_kernel,
        [((own, chans), F32), ((taps_n, chans), F32), ((1, chans), F32)], [VMEM], flops=1 << 22,
        final=True,
    )(packed)
    return (value_grad, gate_grad, taps_grad, gain_grad.reshape(chans), weight_grad)


def solution(mesh):
    shape = (16, 8) if mesh.shape["sp"] == 128 else (mesh.shape["sp"] // 2, 2)
    torus = Mesh(mesh.devices.reshape(*shape, mesh.shape["tp"]), ("z", "y", "tp"))
    placed = (
        P(SP, "tp"),
        P(SP, "tp"),
        P(None, "tp"),
        P("tp"),
        P(None, "tp"),
        P(SP),
        P(SP),
        P(SP, None),
    )

    return jax.shard_map(
        per_device,
        mesh=torus,
        in_specs=placed,
        out_specs=(P(SP, "tp"), P(SP, "tp"), P(None, "tp"), P("tp"), P(SP, "tp")),
        check_vma=False,
    )
```

time: 96.3 us -> 80.4 us (0.83)
  the two profiles are of different devices: /device:TPU:2 before, /device:TPU:8 now
where the time goes in v3:
time: 80.4 us; the launch traced here: 79.9 us
  starting transfers between devices  24.3 us (30%)
  waiting for transfers between devices  23.8 us (30%)
  blocking collectives  21.3 us (26%)
  Pallas kernels  9.81 us (12%)
    all_to_all x1, blocking collectives, exchange(): return lax.all_to_all(value, axis, split_axis=0, concat_axis=0, tiled=True)  21.3 us
    all_to_all x2, starting transfers between devices, exchange(): return lax.all_to_all(value, axis, split_axis=0, concat_axis=0, tiled=True)  17.4 us
    all_to_all x2, waiting for transfers between devices, exchange(): return lax.all_to_all(value, axis, split_axis=0, concat_axis=0, tiled=True)  11.9 us
    ppermute x2, waiting for transfers between devices, passed_along(): return lax.ppermute(value, axis, pairs)  11.9 us
    pallas_call x8, Pallas kernels, with_operands(): run(*(pltpu.with_memory_space_constraint(x, spec.memory_space) for x, spe...  9.81 us
    ppermute x2, starting transfers between devices, passed_along(): return lax.ppermute(value, axis, pairs)  6.85 us
  transfers between devices with their start and end apart: 4, of which 4 were waited for; matrix products, arithmetic and copies ran while one was open for 0% of the time, Pallas kernels for 8%

profile of v3, /device:TPU:8, one launch (start us, length us, event | category | flops | bytes accessed | tf_op | source)
XLA Modules:
  0.0 79.9 jit_solution(16926779105555872052)
XLA Ops:
  0.6 0.7 shard_map.119
  1.4 3.5 %collective-permute-start = (bf16[32,128]{1,0:T(8,128)(2,1)S(1)}, bf16[32,128]{1,0:T(8,128)(2,1)S(1)}, u32[]{:S(2)}, u32[]{:S(2)}) collective-permute-start(bf16[32,128]{1,0:T(8,128)(2,1)S(1)} %shard_map.119), channel_id=1, source_target_pairs={{0,8},{8,16},{16,24},{24,32},{32,40},{40,48},{48,56},{56,64},{64,7... | collective-permute-start | bytes 24584 | tf_op jit(solution)/shard_map/ppermute | solution.py:246
  4.9 2.8 %shard_map.120 = (f32[32,128]{1,0:T(8,128)S(1)}, f32[1,128]{1,0:T(1,128)S(1)}, f32[4,128]{1,0:T(4,128)S(1)}, f32[4,128]{1,0:T(4,128)S(1)}, bf16[512,2048]{1,0:T(...) custom-call(bf16[512,128]{1,0:T(8,128)(2,1)} %value_in.3, ...), custom_call_target="tpu_custom_call" | custom-call | flops 268435456 | tf_op jit(solution)/shard_map/pallas_call | solution.py:265
  7.7 9.6 %collective-permute-done.before_ref = bf16[32,128]{1,0:T(8,128)(2,1)S(1)} collective-permute-done((bf16[32,128]{1,0:T(8,128)(2,1)S(1)}, bf16[32,128]{1,0:T(8,128)(2,1)S(1)}, u32[]{:S(2)}, u32[]{:S(2)}) %collective-permute-start) | collective-permute-done | bytes 8224 | tf_op jit(solution)/shard_map/ppermute | solution.py:246
  17.4 0.8 %shard_map.121 = (f32[32,128]{1,0:T(8,128)S(1)}, f32[32,128]{1,0:T(8,128)S(1)}, bf16[32,128]{1,0:T(8,128)(2,1)S(1)}, f32[8,128]{1,0:T(8,128)S(1)}, f32[8,8,128]{2,1,0:T(8,128)}) custom-call(bf16[32,128]{1,0:T(8,128)(2,1)S(1)} %collective-permute-done.before_ref, f32[32,128]{1,0:T(8,128)S(1)} %get-tuple-element.31.conv_first, ...), custom_call_target="tpu_custom_call" | custom-call | flops 16777216 | tf_op jit(solution)/shard_map/pallas_call | solution.py:265
  18.2 3.3 %all-to-all-start = ((f32[8,8,128]{2,1,0:T(8,128)}), f32[8,8,128]{2,1,0:T(8,128)S(1)}, u32[]{:S(2)}, u32[]{:S(2)}) async-start(f32[8,8,128]{2,1,0:T(8,128)} %get-tuple-element.39), calls=%async_computation | async-start | bytes 65536 | tf_op jit(solution)/shard_map/all_to_all | solution.py:250
  21.5 0.8 shard_map.122.part_ref
  22.3 4.6 %all-to-all-done.all_sums = f32[8,8,128]{2,1,0:T(8,128)S(1)} async-done(((f32[8,8,128]{2,1,0:T(8,128)}), f32[8,8,128]{2,1,0:T(8,128)S(1)}, u32[]{:S(2)}, u32[]{:S(2)}) %all-to-all-start) | async-done | bytes 32800 | tf_op jit(solution)/shard_map/all_to_all | solution.py:250
  26.9 0.9 %shard_map.123 = (bf16[8,288,128]{2,1,0:T(8,128)(2,1)S(1)}, f32[512,128]{1,0:T(8,128)S(1)}, f32[32,128]{1,0:T(8,128)S(1)}) custom-call(f32[8,8,128]{2,1,0:T(8,128)S(1)} %all-to-all-done.all_sums, f32[512,128]{1,0:T(8,128)S(1)} %get-tuple-element.40.centered_ref, f32[512,128]{1,0:T(8,128)S(1)} %get-tuple-element.41.scaled_ref, ...), custom_call_target="tpu_custom_call" | custom-call | flops 67108864 | tf_op jit(solution)/shard_map/pallas_call | solution.py:265
  27.7 21.3 %all_to_all.15.in_ref = bf16[8,288,128]{2,1,0:T(8,128)(2,1)S(1)} all-to-all(bf16[8,288,128]{2,1,0:T(8,128)(2,1)S(1)} %get-tuple-element.53), channel_id=1, replica_groups=mesh['z'=16,'y'=8,'tp'=8] {'y'}, dimensions={0} | all-to-all | bytes 1179648 | tf_op jit(solution)/shard_map/all_to_all | solution.py:250
  49.1 0.8 shard_map.125
  49.8 14.1 %all-to-all-start.2 = ((bf16[16,48,128]{2,1,0:T(8,128)(2,1)}), bf16[16,48,128]{2,1,0:T(8,128)(2,1)S(1)}, u32[]{:S(2)}, u32[]{:S(2)}) async-start(bf16[16,48,128]{2,1,0:T(8,128)(2,1)} %shard_map.125), calls=%async_computation.2 | async-start | bytes 393216 | tf_op jit(solution)/shard_map/all_to_all | solution.py:250
  63.9 3.4 %collective-permute-start.1 = (f32[32,128]{1,0:T(8,128)S(1)}, f32[32,128]{1,0:T(8,128)S(1)}, u32[]{:S(2)}, u32[]{:S(2)}) collective-permute-start(f32[32,128]{1,0:T(8,128)S(1)} %get-tuple-element.50), channel_id=1, source_target_pairs={{8,0},{16,8},{24,16},{32,24},{40,32},{48,40},{56,48},{64,56},{72,6... | collective-permute-start | bytes 49160 | tf_op jit(solution)/shard_map/ppermute | solution.py:246
  67.3 2.3 %collective-permute-done.1.after_ref = f32[32,128]{1,0:T(8,128)S(1)} collective-permute-done((f32[32,128]{1,0:T(8,128)S(1)}, f32[32,128]{1,0:T(8,128)S(1)}, u32[]{:S(2)}, u32[]{:S(2)}) %collective-permute-start.1) | collective-permute-done | bytes 16416 | tf_op jit(solution)/shard_map/ppermute | solution.py:246
  69.5 2.4 %shard_map.124 = (bf16[512,128]{1,0:T(8,128)(2,1)}, bf16[512,128]{1,0:T(8,128)(2,1)}) custom-call(bf16[512,128]{1,0:T(8,128)(2,1)} %value_in.3, bf16[512,128]{1,0:T(8,128)(2,1)} %gate_in.3, f32[512,128]{1,0:T(8,128)S(1)} %get-tuple-element.49.conv_grad_ref, f32[32,128]{1,0:T(8,128)S(1)} %collective-permute-done.1.after_ref, f32[32,128]{1,0:T(8,128)S(1)} %get-tuple-element.33.taps), custom_call_target="tpu_custom_call" | custom-call | flops 268435456 | tf_op jit(solution)/shard_map/pallas_call | solution.py:265
  71.9 7.3 %all-to-all-done.2.in_ref = bf16[16,48,128]{2,1,0:T(8,128)(2,1)S(1)} async-done(((bf16[16,48,128]{2,1,0:T(8,128)(2,1)}), bf16[16,48,128]{2,1,0:T(8,128)(2,1)S(1)}, u32[]{:S(2)}, u32[]{:S(2)}) %all-to-all-start.2) | async-done | bytes 196640 | tf_op jit(solution)/shard_map/all_to_all | solution.py:250
  79.3 0.6 shard_map.126
Async XLA Ops:
  1.4 16.0 %collective-permute-start = (bf16[32,128]{1,0:T(8,128)(2,1)S(1)}, bf16[32,128]{1,0:T(8,128)(2,1)S(1)}, u32[]{:S(2)}, u32[]{:S(2)}) collective-permute-start(bf16[32,128]{1,0:T(8,128)(2,1)S(1)} %shard_map.119), channel_id=1, source_target_pairs={{0,8},{8,16},{16,24},{24,32},{32,40},{40,48},{48,56},{56,64},{64,7... | collective-permute-start | bytes 24584 | tf_op jit(solution)/shard_map/ppermute | solution.py:246
  18.2 8.7 %all-to-all-start = ((f32[8,8,128]{2,1,0:T(8,128)}), f32[8,8,128]{2,1,0:T(8,128)S(1)}, u32[]{:S(2)}, u32[]{:S(2)}) async-start(f32[8,8,128]{2,1,0:T(8,128)} %get-tuple-element.39), calls=%async_computation | async-start | bytes 65536 | tf_op jit(solution)/shard_map/all_to_all | solution.py:250
  49.8 29.5 %all-to-all-start.2 = ((bf16[16,48,128]{2,1,0:T(8,128)(2,1)}), bf16[16,48,128]{2,1,0:T(8,128)(2,1)S(1)}, u32[]{:S(2)}, u32[]{:S(2)}) async-start(bf16[16,48,128]{2,1,0:T(8,128)(2,1)} %shard_map.125), calls=%async_computation.2 | async-start | bytes 393216 | tf_op jit(solution)/shard_map/all_to_all | solution.py:250
  63.9 5.6 %collective-permute-start.1 = (f32[32,128]{1,0:T(8,128)S(1)}, f32[32,128]{1,0:T(8,128)S(1)}, u32[]{:S(2)}, u32[]{:S(2)}) collective-permute-start(f32[32,128]{1,0:T(8,128)S(1)} %get-tuple-element.50), channel_id=1, source_target_pairs={{8,0},{16,8},{24,16},{32,24},{40,32},{48,40},{56,48},{64,56},{72,6... | collective-permute-start | bytes 49160 | tf_op jit(solution)/shard_map/ppermute | solution.py:246

commit v4 on v3

--- a/solution.py
+++ b/solution.py
@@ -57,22 +57,11 @@
 
 
 def main_kernel(
-    value_in, gate_in, taps_in, gain_in, mean_in, scale_in, weight_in, out_grad_in,
-    taps, gain_ref, mean_ref, scale_ref, out_grad_ref,
-    gated_ref, centered_ref, scaled_ref, activated_ref, conv_first, act_first, gain_sum, sums_ref,
-    value_ref, gate_ref, padded, taps_raw, weight_ref, conv_ref, sems,
-):
-    rows, taps_n = value_ref.shape[0], taps_in.shape[0]
-    moved = (
-        (value_in, value_ref), (gate_in, gate_ref), (taps_in, taps_raw), (gain_in, gain_ref),
-        (mean_in, mean_ref), (scale_in, scale_ref), (weight_in, weight_ref),
-        (out_grad_in, out_grad_ref),
-    )
-    copies = [pltpu.make_async_copy(src, dst, sems.at[i]) for i, (src, dst) in enumerate(moved)]
-    for c in copies:
-        c.start()
-    for c in copies[:3]:
-        c.wait()
+    value_ref, gate_ref, taps_raw, gain_ref, mean_ref, scale_ref, weight_ref, out_grad_ref,
+    taps, gated_ref, centered_ref, scaled_ref, activated_ref, conv_first, act_first, gain_sum,
+    sums_ref, padded, conv_ref,
+):
+    rows, taps_n = value_ref.shape[0], taps_raw.shape[0]
     taps[0:taps_n, :] = taps_raw[...].astype(F32)
     gated = (value_ref[...].astype(F32) * jax.nn.sigmoid(gate_ref[...].astype(F32))).astype(BF16)
     gated_ref[...] = gated
@@ -80,8 +69,6 @@
     padded[HALO : HALO + rows, :] = gated.astype(F32)
     for r in range(0, rows, BLOCK):
         conv_ref[r : r + BLOCK, :] = weighted(taps, padded, 2 + r, BLOCK, 1)
-    for c in copies[3:]:
-        c.wait()
     conv_first[...] = conv_ref[0:HALO, :]
     gain = gain_ref[...]
     gain_total = jnp.zeros((8, LANES), F32)
@@ -144,25 +131,35 @@
         sums_out[j] = tile
 
 
-def weight_kernel(out_grad_ref, activated_ref, activated_first, out_ref, *, n_z, n_y):
+def weight_kernel(
+    out_grad_ref, activated_ref, activated_first, keep_ref, send_ref, *, n_z, n_y
+):
     activated = jnp.concatenate([activated_first[...], activated_ref[HALO:, :]], axis=0)
     part = lax.dot_general(
         out_grad_ref[...], activated, (((0,), (0,)), ((), ())), preferred_element_type=F32
-    ).astype(BF16)
+    )
     own = part.shape[0] // (n_z * n_y)
+    half = own // 2
+    even = jnp.full((half, part.shape[1]), lax.axis_index("z") & 1, jnp.int32) == 0
     for z in range(n_z):
         for y in range(n_y):
             at = (z * n_y + y) * own
-            out_ref[y, z * own : (z + 1) * own, :] = part[at : at + own]
+            upper, lower = part[at : at + half], part[at + half : at + own]
+            keep_ref[y, z * half : (z + 1) * half, :] = jnp.where(even, upper, lower)
+            send_ref[y, z * half : (z + 1) * half, :] = jnp.where(even, lower, upper).astype(BF16)
 
 
 def pack_kernel(
     all_sums, centered_ref, scaled_ref, centered_first, scaled_first, gated_ref, before_ref,
-    scale_ref, part_ref, gain_sum,
-    out_ref, conv_grad_ref, first_rows, padded,
+    scale_ref, keep_ref, sent_ref, gain_sum, value_in, gate_in,
+    out_ref, conv_grad_ref, first_rows, value_ref, gate_ref, padded, sems,
     *, channels, taps_n,
 ):
     rows = gated_ref.shape[0]
+    moved = ((value_in, value_ref), (gate_in, gate_ref))
+    copies = [pltpu.make_async_copy(src, dst, sems.at[i]) for i, (src, dst) in enumerate(moved)]
+    for c in copies:
+        c.start()
     tile = all_sums[0]
     for j in range(1, all_sums.shape[0]):
         tile = tile + all_sums[j]
@@ -191,47 +188,47 @@
         small += [jnp.sum(totals[k], axis=0, keepdims=True) for k in ks]
     small.append(jnp.sum(gain_sum[...], axis=0, keepdims=True))
     small = jnp.concatenate(small, axis=0).astype(BF16)
-    big = part_ref.shape[1]
+    big = keep_ref.shape[1]
     for y in range(out_ref.shape[0]):
-        out_ref[y, 0:big, :] = part_ref[y]
+        out_ref[y, 0:big, :] = (keep_ref[y] + sent_ref[y].astype(F32)).astype(BF16)
         out_ref[y, big : big + taps_n + 1, :] = small
-
-
-def middle_kernel(in_ref, out_ref, *, own):
+    for c in copies:
+        c.wait()
+
+
+def middle_kernel(in_ref, out_ref, *, half):
     total = in_ref[0].astype(F32)
     for y in range(1, in_ref.shape[0]):
         total = total + in_ref[y].astype(F32)
-    total = total.astype(BF16)
     n_z = out_ref.shape[0]
-    small = total[n_z * own :]
+    small = total[n_z * half :].astype(BF16)
     for z in range(n_z):
-        out_ref[z, 0:own, :] = total[z * own : (z + 1) * own]
-        out_ref[z, own:, :] = small
+        out_ref[z, 0:half, :] = total[z * half : (z + 1) * half].astype(BF16)
+        out_ref[z, half:, :] = small
 
 
 def last_kernel(in_ref, weight_ref, taps_ref, gain_ref):
-    total = in_ref[0].astype(F32)
-    for z in range(1, in_ref.shape[0]):
-        total = total + in_ref[z].astype(F32)
-    own, taps_n = weight_ref.shape[0], taps_ref.shape[0]
-    weight_ref[...] = total[0:own]
-    taps_ref[...] = total[own : own + taps_n]
-    gain_ref[...] = total[own + taps_n : own + taps_n + 1]
+    half, taps_n = weight_ref.shape[0] // 2, taps_ref.shape[0]
+    big, small = [], None
+    for z in range(in_ref.shape[0]):
+        block = in_ref[z].astype(F32)
+        if z < 2:
+            big.append(block[:half])
+        else:
+            big[z % 2] = big[z % 2] + block[:half]
+        small = block[half:] if small is None else small + block[half:]
+    weight_ref[0:half, :] = big[0]
+    weight_ref[half:, :] = big[1]
+    taps_ref[...] = small[0:taps_n]
+    gain_ref[...] = small[taps_n : taps_n + 1]
 
 
 def glu_kernel(
-    value_in, gate_in, conv_grad_ref, after_ref, taps, value_grad, gate_grad,
-    value_ref, gate_ref, padded, sems,
+    value_ref, gate_ref, conv_grad_ref, after_ref, taps, value_grad, gate_grad, padded
 ):
     rows, taps_n = value_ref.shape[0], taps.shape[0] - 1
-    moved = ((value_in, value_ref), (gate_in, gate_ref))
-    copies = [pltpu.make_async_copy(src, dst, sems.at[i]) for i, (src, dst) in enumerate(moved)]
-    for c in copies:
-        c.start()
     padded[0:rows, :] = conv_grad_ref[...]
     padded[rows : rows + HALO, :] = after_ref[...]
-    for c in copies:
-        c.wait()
     for r in range(0, rows, BLOCK):
         gated_grad = weighted(taps, padded, r + taps_n - 1, BLOCK, -1)
         sig = jax.nn.sigmoid(gate_ref[r : r + BLOCK, :].astype(F32))
@@ -280,6 +277,7 @@
     wide = out_grad.shape[1]
     n_z, n_y, n_tp = lax.axis_size("z"), lax.axis_size("y"), lax.axis_size("tp")
     own = wide // (n_z * n_y)
+    half = own // 2
     n_b = rows // LANES
     gain = norm_gain.reshape(1, chans)
     mean, scale = norm_mean.reshape(n_b, LANES), norm_scale.reshape(n_b, LANES)
@@ -288,20 +286,15 @@
     (tail,) = call(
         tail_kernel, [(few, BF16)], [HBM, HBM],
         [pltpu.VMEM(few, BF16), pltpu.VMEM(few, BF16), pltpu.SemaphoreType.DMA((2,))],
+        flops=1 << 30,
     )(glu_value, glu_gate)
     before = passed_along(tail, SP, 1)
-    block = (n_b, LANES)
-    (taps, gain, mean, scale, out_grad_here,
-     gated, centered, scaled, activated, conv0, act0, gain_sum, sums) = call(
+    (taps, gated, centered, scaled, activated, conv0, act0, gain_sum, sums) = call(
         main_kernel,
-        [((taps_n + 1, chans), F32), ((1, chans), F32), (block, F32),
-         (block, F32), ((rows, wide), BF16),
-         (full, BF16), (full, F32), (full, F32), (full, BF16), (few, F32), (few, F32),
-         ((8, chans), F32), ((2 * n_b, LANES), F32)],
-        [HBM] * 8,
-        [pltpu.VMEM(full, BF16), pltpu.VMEM(full, BF16),
-         pltpu.VMEM((HALO + rows, chans), F32), pltpu.VMEM((taps_n, chans), BF16),
-         pltpu.VMEM((wide, chans), BF16), pltpu.VMEM(full, F32), pltpu.SemaphoreType.DMA((8,))],
+        [((taps_n + 1, chans), F32), (full, BF16), (full, F32), (full, F32), (full, BF16),
+         (few, F32), (few, F32), ((8, chans), F32), ((2 * n_b, LANES), F32)],
+        [VMEM] * 8,
+        [pltpu.VMEM((HALO + rows, chans), F32), pltpu.VMEM(full, F32)],
         flops=1 << 28,
     )(glu_value, glu_gate, conv_taps, gain, mean, scale, out_weight, out_grad)
     centered0, scaled0, activated0, gain_sum, sums = call(
@@ -311,30 +304,33 @@
         [pltpu.VMEM((2 * HALO, chans), F32)],
         flops=1 << 24,
     )(before, conv0, act0, taps, gain, mean, scale, gain_sum, sums)
+    keep, send = call(
+        functools.partial(weight_kernel, n_z=n_z, n_y=n_y),
+        [((n_y, n_z * half, chans), F32), ((n_y, n_z * half, chans), BF16)],
+        [VMEM] * 3, flops=1 << 28,
+    )(out_grad, activated, activated0)
+    sent = lax.ppermute(send, "z", [(i, i ^ 1) for i in range(n_z)])
     sums = exchange(sums, "tp")
-    (part,) = call(
-        functools.partial(weight_kernel, n_z=n_z, n_y=n_y),
-        [((n_y, n_z * own, chans), BF16)], [VMEM] * 3, flops=1 << 28,
-    )(out_grad_here, activated, activated0)
-    packed, conv_grad, first_rows = call(
+    packed, conv_grad, first_rows, value, gate = call(
         functools.partial(pack_kernel, channels=chans * n_tp, taps_n=taps_n),
-        [((n_y, n_z * own + taps_n + 1, chans), BF16), (full, F32), (few, F32)],
-        [VMEM] * 10,
-        [pltpu.VMEM((HALO + rows, chans), F32)],
+        [((n_y, n_z * half + taps_n + 1, chans), BF16), (full, F32), (few, F32), (full, BF16),
+         (full, BF16)],
+        [VMEM] * 11 + [HBM] * 2,
+        [pltpu.VMEM((HALO + rows, chans), F32), pltpu.SemaphoreType.DMA((2,))],
         flops=1 << 26,
-    )(sums, centered, scaled, centered0, scaled0, gated, before, scale, part, gain_sum)
+    )(sums, centered, scaled, centered0, scaled0, gated, before, scale, keep, sent, gain_sum,
+      glu_value, glu_gate)
     packed = exchange(packed, "y")
     (packed,) = call(
-        functools.partial(middle_kernel, own=own),
-        [((n_z, own + taps_n + 1, chans), BF16)], [VMEM], flops=1 << 22,
+        functools.partial(middle_kernel, half=half),
+        [((n_z, half + taps_n + 1, chans), BF16)], [VMEM], flops=1 << 22,
     )(packed)
     packed = exchange(packed, "z")
     after = passed_along(first_rows, SP, -1)
     value_grad, gate_grad = call(
-        glu_kernel, [(full, BF16), (full, BF16)], [HBM] * 2 + [VMEM] * 3,
-        [pltpu.VMEM(full, BF16), pltpu.VMEM(full, BF16), pltpu.VMEM((rows + HALO, chans), F32),
-         pltpu.SemaphoreType.DMA((2,))], flops=1 << 28, final=True,
-    )(glu_value, glu_gate, conv_grad, after, taps)
+        glu_kernel, [(full, BF16), (full, BF16)], [VMEM] * 5,
+        [pltpu.VMEM((rows + HALO, chans), F32)], flops=1 << 28, final=True,
+    )(value, gate, conv_grad, after, taps)
     weight_grad, taps_grad, gain_grad = call(
         last_kernel,
         [((own, chans), F32), ((taps_n, chans), F32), ((1, chans), F32)], [VMEM], flops=1 << 22,

time: 80.4 us -> 77.4 us (0.963)
  the two profiles are of different devices: /device:TPU:8 before, /device:TPU:2 now
where the time goes in v4:
time: 77.4 us; the launch traced here: 76.9 us
  blocking collectives  28.7 us (37%)
  starting transfers between devices  28.6 us (37%)
  waiting for transfers between devices  11.6 us (15%)
  Pallas kernels  7.14 us (9%)
  between operations  0.83 us (1%)
    all_to_all x2, blocking collectives, exchange(): return lax.all_to_all(value, axis, split_axis=0, concat_axis=0, tiled=True)  28.7 us
    all_to_all x1, starting transfers between devices, exchange(): return lax.all_to_all(value, axis, split_axis=0, concat_axis=0, tiled=True)  17.1 us
    all_to_all x1, waiting for transfers between devices, exchange(): return lax.all_to_all(value, axis, split_axis=0, concat_axis=0, tiled=True)  7.24 us
    pallas_call x8, Pallas kernels, with_operands(): run(*(pltpu.with_memory_space_constraint(x, spec.memory_space) for x, spe...  7.14 us
    ppermute x1, starting transfers between devices, per_device(): sent = lax.ppermute(send, 'z', [(i, i ^ 1) for i in range(n_z)])  6.79 us
    ppermute x2, starting transfers between devices, passed_along(): return lax.ppermute(value, axis, pairs)  4.77 us
    ppermute x2, waiting for transfers between devices, passed_along(): return lax.ppermute(value, axis, pairs)  4.34 us
  transfers between devices with their start and end apart: 4, of which 2 were waited for; matrix products, arithmetic and copies ran while one was open for 0% of the time, Pallas kernels for 4%

profile of v4, /device:TPU:2, one launch (start us, length us, event | category | flops | bytes accessed | tf_op | source)
XLA Modules:
  0.0 76.9 jit_solution(11754727426183560669)
XLA Ops:
  0.6 0.0 copy-start.3
  0.6 0.0 copy-start.2
  0.7 0.0 copy-start
  0.7 0.0 copy-start.4
  0.7 0.0 copy-start.6
  0.7 0.0 copy-start.1
  0.7 0.0 copy-start.7
  0.7 0.0 copy-start.5
  0.7 0.9 %shard_map.119 = bf16[32,128]{1,0:T(8,128)(2,1)S(1)} custom-call(bf16[512,128]{1,0:T(8,128)(2,1)} %value_in.1, bf16[512,128]{1,0:T(8,128)(2,1)} %gate_in.1), custom_call_target="tpu_custom_call" | custom-call | flops 1073741824 | tf_op jit(solution)/shard_map/pallas_call | solution.py:262
  1.6 3.5 %collective-permute-start = (bf16[32,128]{1,0:T(8,128)(2,1)S(1)}, bf16[32,128]{1,0:T(8,128)(2,1)S(1)}, u32[]{:S(2)}, u32[]{:S(2)}) collective-permute-start(bf16[32,128]{1,0:T(8,128)(2,1)S(1)} %shard_map.119), channel_id=1, source_target_pairs={{0,8},{8,16},{16,24},{24,32},{32,40},{40,48},{48,56},{56,64},{64,7... | collective-permute-start | bytes 24584 | tf_op jit(solution)/shard_map/ppermute | solution.py:243
  5.1 0.0 copy-done.3
  5.1 0.0 copy-done.2
  5.1 0.0 copy-done
  5.1 0.0 copy-done.4
  5.1 0.0 copy-done.6
  5.2 0.0 copy-done.1
  5.2 0.0 copy-done.7
  5.2 0.0 copy-done.5
  5.2 1.6 %shard_map.120 = (f32[32,128]{1,0:T(8,128)S(1)}, bf16[512,128]{1,0:T(8,128)(2,1)S(1)}, f32[512,128]{1,0:T(8,128)S(1)}, f32[512,128]{1,0:T(8,128)S(1)}, bf16[512,...) custom-call(bf16[512,128]{1,0:T(8,128)(2,1)S(1)} %copy-done.2, ...), custom_call_target="tpu_custom_call" | custom-call | flops 268435456 | tf_op jit(solution)/shard_map/pallas_call | solution.py:262
  6.8 0.0 collective-permute-done.before_ref
  6.8 0.2 shard_map.121
  7.0 0.8 %shard_map.122 = (f32[8,128,128]{2,1,0:T(8,128)S(1)}, bf16[8,128,128]{2,1,0:T(8,128)(2,1)S(1)}) custom-call(bf16[512,2048]{1,0:T(8,128)(2,1)S(1)} %copy-done, bf16[512,128]{1,0:T(8,128)(2,1)S(1)} %get-tuple-element.42.activated_ref, bf16[32,128]{1,0:T(8,128)(2,1)S(1)} %get-tuple-element.43.activated_first), custom_call_target="tpu_custom_call" | custom-call | flops 268435456 | tf_op jit(solution)/shard_map/pallas_call | solution.py:262
  7.8 6.8 %collective-permute-start.1 = (bf16[8,128,128]{2,1,0:T(8,128)(2,1)S(1)}, bf16[8,128,128]{2,1,0:T(8,128)(2,1)S(1)}, u32[]{:S(2)}, u32[]{:S(2)}) collective-permute-start(bf16[8,128,128]{2,1,0:T(8,128)(2,1)S(1)} %get-tuple-element.45), channel_id=1, source_target_pairs={{0,64},{64,0},{128,192},{192,128},{256,320},{320,256},{384,448},{4... | collective-permute-start | bytes 786440 | tf_op jit(solution)/shard_map/ppermute | solution.py:312
  14.6 12.5 %all_to_all.15.all_sums = f32[8,8,128]{2,1,0:T(8,128)S(1)} all-to-all(f32[8,8,128]{2,1,0:T(8,128)S(1)} %get-tuple-element.36), channel_id=1, replica_groups=mesh['z'=16,'y'=8,'tp'=8] {'tp'}, dimensions={0} | all-to-all | bytes 65536 | tf_op jit(solution)/shard_map/all_to_all | solution.py:247
  27.0 0.0 collective-permute-done.1.sent_ref
  27.0 1.0 %shard_map.123 = (bf16[8,160,128]{2,1,0:T(8,128)(2,1)S(1)}, f32[512,128]{1,0:T(8,128)S(1)}, f32[32,128]{1,0:T(8,128)S(1)}, bf16[512,128]{1,0:T(8,128)(2,1)S(1)}, bf16[512,128]{1,0:T(8,128)(2,1)S(1)}) custom-call(f32[8,8,128]{2,1,0:T(8,128)S(1)} %all_to_all.15.all_sums, f32[512,128]{1,0:T(8,128)S(1)} %get-tuple-element.37.centered_ref, ...), custom_call_target="tpu_custom_call" | custom-call | flops 67108864 | tf_op jit(solution)/shard_map/pallas_call | solution.py:262
  28.0 16.3 %all_to_all.16.in_ref = bf16[8,160,128]{2,1,0:T(8,128)(2,1)S(1)} all-to-all(bf16[8,160,128]{2,1,0:T(8,128)(2,1)S(1)} %get-tuple-element.53), channel_id=1, replica_groups=mesh['z'=16,'y'=8,'tp'=8] {'y'}, dimensions={0} | all-to-all | bytes 655360 | tf_op jit(solution)/shard_map/all_to_all | solution.py:247
  44.3 0.7 shard_map.125
  45.0 17.1 %all-to-all-start.2 = ((bf16[16,40,128]{2,1,0:T(8,128)(2,1)}), bf16[16,40,128]{2,1,0:T(8,128)(2,1)S(1)}, u32[]{:S(2)}, u32[]{:S(2)}) async-start(bf16[16,40,128]{2,1,0:T(8,128)(2,1)} %shard_map.125), calls=%async_computation.2 | async-start | bytes 327680 | tf_op jit(solution)/shard_map/all_to_all | solution.py:247
  62.1 1.3 %collective-permute-start.2 = (f32[32,128]{1,0:T(8,128)S(1)}, f32[32,128]{1,0:T(8,128)S(1)}, u32[]{:S(2)}, u32[]{:S(2)}) collective-permute-start(f32[32,128]{1,0:T(8,128)S(1)} %get-tuple-element.50), channel_id=1, source_target_pairs={{8,0},{16,8},{24,16},{32,24},{40,32},{48,40},{56,48},{64,56},{72,6... | collective-permute-start | bytes 49160 | tf_op jit(solution)/shard_map/ppermute | solution.py:243
  63.4 4.3 %collective-permute-done.2.after_ref = f32[32,128]{1,0:T(8,128)S(1)} collective-permute-done((f32[32,128]{1,0:T(8,128)S(1)}, f32[32,128]{1,0:T(8,128)S(1)}, u32[]{:S(2)}, u32[]{:S(2)}) %collective-permute-start.2) | collective-permute-done | bytes 16416 | tf_op jit(solution)/shard_map/ppermute | solution.py:243
  67.7 1.3 %shard_map.124 = (bf16[512,128]{1,0:T(8,128)(2,1)}, bf16[512,128]{1,0:T(8,128)(2,1)}) custom-call(bf16[512,128]{1,0:T(8,128)(2,1)S(1)} %get-tuple-element.47.value_ref, bf16[512,128]{1,0:T(8,128)(2,1)S(1)} %get-tuple-element.48.gate_ref, f32[512,128]{1,0:T(8,128)S(1)} %get-tuple-element.49.conv_grad_ref, f32[32,128]{1,0:T(8,128)S(1)} %collective-permute-done.2.after_ref, ...), custom_call_target="tpu_custom_call" | custom-call | flops 268435456 | tf_op jit(solution)/shard_map/pallas_call | solution.py:262
  69.1 7.2 %all-to-all-done.2.in_ref = bf16[16,40,128]{2,1,0:T(8,128)(2,1)S(1)} async-done(((bf16[16,40,128]{2,1,0:T(8,128)(2,1)}), bf16[16,40,128]{2,1,0:T(8,128)(2,1)S(1)}, u32[]{:S(2)}, u32[]{:S(2)}) %all-to-all-start.2) | async-done | bytes 163872 | tf_op jit(solution)/shard_map/all_to_all | solution.py:247
  76.3 0.6 shard_map.126
Async XLA Ops:
  0.6 4.5 %copy-start.3 = (bf16[512,128]{1,0:T(8,128)(2,1)S(1)}, bf16[512,128]{1,0:T(8,128)(2,1)}, u32[]{:S(2)}) copy-start(bf16[512,128]{1,0:T(8,128)(2,1)} %gate_in.1) | copy-start | bytes 393220
  0.6 4.5 %copy-start.2 = (bf16[512,128]{1,0:T(8,128)(2,1)S(1)}, bf16[512,128]{1,0:T(8,128)(2,1)}, u32[]{:S(2)}) copy-start(bf16[512,128]{1,0:T(8,128)(2,1)} %value_in.1) | copy-start | bytes 393220
  0.7 4.5 %copy-start = (bf16[512,2048]{1,0:T(8,128)(2,1)S(1)}, bf16[512,2048]{1,0:T(8,128)(2,1)}, u32[]{:S(2)}) copy-start(bf16[512,2048]{1,0:T(8,128)(2,1)} %out_grad_ref.3) | copy-start | bytes 6291460
  0.7 4.5 %copy-start.4 = (f32[512]{0:T(512)S(1)}, f32[512]{0:T(512)}, u32[]{:S(2)}) copy-start(f32[512]{0:T(512)} %param.14) | copy-start | bytes 6148
  0.7 4.5 %copy-start.6 = (f32[512]{0:T(512)S(1)}, f32[512]{0:T(512)}, u32[]{:S(2)}) copy-start(f32[512]{0:T(512)} %param.13) | copy-start | bytes 6148
  0.7 4.5 %copy-start.1 = (bf16[2048,128]{1,0:T(8,128)(2,1)S(1)}, bf16[2048,128]{1,0:T(8,128)(2,1)}, u32[]{:S(2)}) copy-start(bf16[2048,128]{1,0:T(8,128)(2,1)} %weight_ref.1) | copy-start | bytes 1572868
  0.7 4.5 %copy-start.7 = (f32[128]{0:T(128)S(1)}, f32[128]{0:T(128)}, u32[]{:S(2)}) copy-start(f32[128]{0:T(128)} %param.11) | copy-start | bytes 1540
  0.7 4.5 %copy-start.5 = (bf16[31,128]{1,0:T(8,128)(2,1)S(1)}, bf16[31,128]{1,0:T(8,128)(2,1)}, u32[]{:S(2)}) copy-start(bf16[31,128]{1,0:T(8,128)(2,1)} %taps_raw.1) | copy-start | bytes 23812
  1.6 5.1 %collective-permute-start = (bf16[32,128]{1,0:T(8,128)(2,1)S(1)}, bf16[32,128]{1,0:T(8,128)(2,1)S(1)}, u32[]{:S(2)}, u32[]{:S(2)}) collective-permute-start(bf16[32,128]{1,0:T(8,128)(2,1)S(1)} %shard_map.119), channel_id=1, source_target_pairs={{0,8},{8,16},{16,24},{24,32},{32,40},{40,48},{48,56},{56,64},{64,7... | collective-permute-start | bytes 24584 | tf_op jit(solution)/shard_map/ppermute | solution.py:243
  7.8 19.3 %collective-permute-start.1 = (bf16[8,128,128]{2,1,0:T(8,128)(2,1)S(1)}, bf16[8,128,128]{2,1,0:T(8,128)(2,1)S(1)}, u32[]{:S(2)}, u32[]{:S(2)}) collective-permute-start(bf16[8,128,128]{2,1,0:T(8,128)(2,1)S(1)} %get-tuple-element.45), channel_id=1, source_target_pairs={{0,64},{64,0},{128,192},{192,128},{256,320},{320,256},{384,448},{4... | collective-permute-start | bytes 786440 | tf_op jit(solution)/shard_map/ppermute | solution.py:312
  45.0 31.3 %all-to-all-start.2 = ((bf16[16,40,128]{2,1,0:T(8,128)(2,1)}), bf16[16,40,128]{2,1,0:T(8,128)(2,1)S(1)}, u32[]{:S(2)}, u32[]{:S(2)}) async-start(bf16[16,40,128]{2,1,0:T(8,128)(2,1)} %shard_map.125), calls=%async_computation.2 | async-start | bytes 327680 | tf_op jit(solution)/shard_map/all_to_all | solution.py:247
  62.1 5.6 %collective-permute-start.2 = (f32[32,128]{1,0:T(8,128)S(1)}, f32[32,128]{1,0:T(8,128)S(1)}, u32[]{:S(2)}, u32[]{:S(2)}) collective-permute-start(f32[32,128]{1,0:T(8,128)S(1)} %get-tuple-element.50), channel_id=1, source_target_pairs={{8,0},{16,8},{24,16},{32,24},{40,32},{48,40},{56,48},{64,56},{72,6... | collective-permute-start | bytes 49160 | tf_op jit(solution)/shard_map/ppermute | solution.py:243

commit v5 on v4

--- a/solution.py
+++ b/solution.py
@@ -12,6 +12,7 @@
 HALO = 32
 BLOCK = 64
 LANES = 128
+Z_FIRST, Y_FIRST, TP_FIRST = 9, 4, 5
 F32, BF16 = jnp.float32, jnp.bfloat16
 VMEM = pl.BlockSpec(memory_space=pltpu.VMEM)
 HBM = pl.BlockSpec(memory_space=pltpu.HBM)
@@ -153,7 +154,7 @@
     all_sums, centered_ref, scaled_ref, centered_first, scaled_first, gated_ref, before_ref,
     scale_ref, keep_ref, sent_ref, gain_sum, value_in, gate_in,
     out_ref, conv_grad_ref, first_rows, value_ref, gate_ref, padded, sems,
-    *, channels, taps_n,
+    *, channels, taps_n, order,
 ):
     rows = gated_ref.shape[0]
     moved = ((value_in, value_ref), (gate_in, gate_ref))
@@ -189,33 +190,30 @@
     small.append(jnp.sum(gain_sum[...], axis=0, keepdims=True))
     small = jnp.concatenate(small, axis=0).astype(BF16)
     big = keep_ref.shape[1]
-    for y in range(out_ref.shape[0]):
-        out_ref[y, 0:big, :] = (keep_ref[y] + sent_ref[y].astype(F32)).astype(BF16)
-        out_ref[y, big : big + taps_n + 1, :] = small
+    for j, y in enumerate(order):
+        out_ref[j, 0:big, :] = (keep_ref[y] + sent_ref[y].astype(F32)).astype(BF16)
+        out_ref[j, big : big + taps_n + 1, :] = small
     for c in copies:
         c.wait()
 
 
-def middle_kernel(in_ref, out_ref, *, half):
+def middle_kernel(in_ref, out_ref, *, half, order):
     total = in_ref[0].astype(F32)
     for y in range(1, in_ref.shape[0]):
         total = total + in_ref[y].astype(F32)
-    n_z = out_ref.shape[0]
-    small = total[n_z * half :].astype(BF16)
-    for z in range(n_z):
-        out_ref[z, 0:half, :] = total[z * half : (z + 1) * half].astype(BF16)
-        out_ref[z, half:, :] = small
-
-
-def last_kernel(in_ref, weight_ref, taps_ref, gain_ref):
+    small = total[len(order) * half :].astype(BF16)
+    for j, z in enumerate(order):
+        out_ref[j, 0:half, :] = total[z * half : (z + 1) * half].astype(BF16)
+        out_ref[j, half:, :] = small
+
+
+def last_kernel(in_ref, weight_ref, taps_ref, gain_ref, *, order):
     half, taps_n = weight_ref.shape[0] // 2, taps_ref.shape[0]
-    big, small = [], None
-    for z in range(in_ref.shape[0]):
-        block = in_ref[z].astype(F32)
-        if z < 2:
-            big.append(block[:half])
-        else:
-            big[z % 2] = big[z % 2] + block[:half]
+    big, small = [None, None], None
+    for j, z in enumerate(order):
+        block = in_ref[j].astype(F32)
+        own = big[z % 2]
+        big[z % 2] = block[:half] if own is None else own + block[:half]
         small = block[half:] if small is None else small + block[half:]
     weight_ref[0:half, :] = big[0]
     weight_ref[half:, :] = big[1]
@@ -243,8 +241,14 @@
     return lax.ppermute(value, axis, pairs)
 
 
-def exchange(value, axis):
-    return lax.all_to_all(value, axis, split_axis=0, concat_axis=0, tiled=True)
+def listed(length, first):
+    return tuple((first + i) % length for i in range(length))
+
+
+def exchange(value, axis, order):
+    return lax.all_to_all(
+        value, axis, split_axis=0, concat_axis=0, tiled=True, axis_index_groups=[list(order)]
+    )
 
 
 def call(kernel, outs, in_specs, scratch=(), flops=0, final=False):
@@ -278,6 +282,8 @@
     n_z, n_y, n_tp = lax.axis_size("z"), lax.axis_size("y"), lax.axis_size("tp")
     own = wide // (n_z * n_y)
     half = own // 2
+    order_z, order_y = listed(n_z, n_z * Z_FIRST // 16), listed(n_y, n_y * Y_FIRST // 8)
+    order_tp = listed(n_tp, n_tp * TP_FIRST // 8)
     n_b = rows // LANES
     gain = norm_gain.reshape(1, chans)
     mean, scale = norm_mean.reshape(n_b, LANES), norm_scale.reshape(n_b, LANES)
@@ -310,9 +316,9 @@
         [VMEM] * 3, flops=1 << 28,
     )(out_grad, activated, activated0)
     sent = lax.ppermute(send, "z", [(i, i ^ 1) for i in range(n_z)])
-    sums = exchange(sums, "tp")
+    sums = exchange(sums, "tp", order_tp)
     packed, conv_grad, first_rows, value, gate = call(
-        functools.partial(pack_kernel, channels=chans * n_tp, taps_n=taps_n),
+        functools.partial(pack_kernel, channels=chans * n_tp, taps_n=taps_n, order=order_y),
         [((n_y, n_z * half + taps_n + 1, chans), BF16), (full, F32), (few, F32), (full, BF16),
          (full, BF16)],
         [VMEM] * 11 + [HBM] * 2,
@@ -320,19 +326,19 @@
         flops=1 << 26,
     )(sums, centered, scaled, centered0, scaled0, gated, before, scale, keep, sent, gain_sum,
       glu_value, glu_gate)
-    packed = exchange(packed, "y")
+    packed = exchange(packed, "y", order_y)
     (packed,) = call(
-        functools.partial(middle_kernel, half=half),
+        functools.partial(middle_kernel, half=half, order=order_z),
         [((n_z, half + taps_n + 1, chans), BF16)], [VMEM], flops=1 << 22,
     )(packed)
-    packed = exchange(packed, "z")
+    packed = exchange(packed, "z", order_z)
     after = passed_along(first_rows, SP, -1)
     value_grad, gate_grad = call(
         glu_kernel, [(full, BF16), (full, BF16)], [VMEM] * 5,
         [pltpu.VMEM((rows + HALO, chans), F32)], flops=1 << 28, final=True,
     )(value, gate, conv_grad, after, taps)
     weight_grad, taps_grad, gain_grad = call(
-        last_kernel,
+        functools.partial(last_kernel, order=order_z),
         [((own, chans), F32), ((taps_n, chans), F32), ((1, chans), F32)], [VMEM], flops=1 << 22,
         final=True,
     )(packed)

time: 77.4 us -> 72.6 us (0.938)
  the two profiles are of different devices: /device:TPU:2 before, /device:TPU:56 now
where the time goes in v5:
time: 72.6 us; the launch traced here: 72.2 us
  starting transfers between devices  29.4 us (40%)
  blocking collectives  29 us (40%)
  Pallas kernels  7.13 us (10%)
  waiting for transfers between devices  5.75 us (8%)
  between operations  0.82 us (1%)
    all_to_all x2, blocking collectives, exchange(): lax.all_to_all(value, axis, split_axis=0, concat_axis=0, tiled=True, axis...  29 us
    all_to_all x1, starting transfers between devices, exchange(): lax.all_to_all(value, axis, split_axis=0, concat_axis=0, tiled=True, axis...  18.2 us
    pallas_call x8, Pallas kernels, with_operands(): run(*(pltpu.with_memory_space_constraint(x, spec.memory_space) for x, spe...  7.13 us
    ppermute x2, starting transfers between devices, passed_along(): return lax.ppermute(value, axis, pairs)  6.93 us
    ppermute x2, waiting for transfers between devices, passed_along(): return lax.ppermute(value, axis, pairs)  5.74 us
    ppermute x1, starting transfers between devices, per_device(): sent = lax.ppermute(send, 'z', [(i, i ^ 1) for i in range(n_z)])  4.28 us
  transfers between devices with their start and end apart: 4, of which 2 were waited for; matrix products, arithmetic and copies ran while one was open for 0% of the time, Pallas kernels for 4%

profile of v5, /device:TPU:56, one launch (start us, length us, event | category | flops | bytes accessed | tf_op | source)
XLA Modules:
  0.0 72.2 jit_solution(12403058233343817060)
XLA Ops:
  0.6 0.0 copy-start.3
  0.6 0.0 copy-start.2
  0.7 0.0 copy-start
  0.7 0.0 copy-start.4
  0.7 0.0 copy-start.6
  0.7 0.0 copy-start.1
  0.7 0.0 copy-start.7
  0.7 0.0 copy-start.5
  0.7 0.9 %shard_map.119 = bf16[32,128]{1,0:T(8,128)(2,1)S(1)} custom-call(bf16[512,128]{1,0:T(8,128)(2,1)} %value_in.1, bf16[512,128]{1,0:T(8,128)(2,1)} %gate_in.1), custom_call_target="tpu_custom_call" | custom-call | flops 1073741824 | tf_op jit(solution)/shard_map/pallas_call | solution.py:266
  1.6 3.5 %collective-permute-start = (bf16[32,128]{1,0:T(8,128)(2,1)S(1)}, bf16[32,128]{1,0:T(8,128)(2,1)S(1)}, u32[]{:S(2)}, u32[]{:S(2)}) collective-permute-start(bf16[32,128]{1,0:T(8,128)(2,1)S(1)} %shard_map.119), channel_id=1, source_target_pairs={{0,8},{8,16},{16,24},{24,32},{32,40},{40,48},{48,56},{56,64},{64,7... | collective-permute-start | bytes 24584 | tf_op jit(solution)/shard_map/ppermute | solution.py:241
  5.1 0.0 copy-done.3
  5.1 0.0 copy-done.2
  5.1 0.0 copy-done
  5.1 0.0 copy-done.4
  5.2 0.0 copy-done.6
  5.2 0.0 copy-done.1
  5.2 0.0 copy-done.7
  5.2 0.0 copy-done.5
  5.2 1.6 %shard_map.120 = (f32[32,128]{1,0:T(8,128)S(1)}, bf16[512,128]{1,0:T(8,128)(2,1)S(1)}, f32[512,128]{1,0:T(8,128)S(1)}, f32[512,128]{1,0:T(8,128)S(1)}, bf16[512,...) custom-call(bf16[512,128]{1,0:T(8,128)(2,1)S(1)} %copy-done.2, ...), custom_call_target="tpu_custom_call" | custom-call | flops 268435456 | tf_op jit(solution)/shard_map/pallas_call | solution.py:266
  6.8 0.4 collective-permute-done.before_ref
  7.2 0.2 shard_map.121
  7.4 0.8 %shard_map.122 = (f32[8,128,128]{2,1,0:T(8,128)S(1)}, bf16[8,128,128]{2,1,0:T(8,128)(2,1)S(1)}) custom-call(bf16[512,2048]{1,0:T(8,128)(2,1)S(1)} %copy-done, bf16[512,128]{1,0:T(8,128)(2,1)S(1)} %get-tuple-element.42.activated_ref, bf16[32,128]{1,0:T(8,128)(2,1)S(1)} %get-tuple-element.43.activated_first), custom_call_target="tpu_custom_call" | custom-call | flops 268435456 | tf_op jit(solution)/shard_map/pallas_call | solution.py:266
  8.2 4.3 %collective-permute-start.1 = (bf16[8,128,128]{2,1,0:T(8,128)(2,1)S(1)}, bf16[8,128,128]{2,1,0:T(8,128)(2,1)S(1)}, u32[]{:S(2)}, u32[]{:S(2)}) collective-permute-start(bf16[8,128,128]{2,1,0:T(8,128)(2,1)S(1)} %get-tuple-element.45), channel_id=1, source_target_pairs={{0,64},{64,0},{128,192},{192,128},{256,320},{320,256},{384,448},{4... | collective-permute-start | bytes 786440 | tf_op jit(solution)/shard_map/ppermute | solution.py:318
  12.5 7.4 %all_to_all.15.all_sums = f32[8,8,128]{2,1,0:T(8,128)S(1)} all-to-all(f32[8,8,128]{2,1,0:T(8,128)S(1)} %get-tuple-element.36), channel_id=1, replica_groups={{5,6,7,0,1,2,3,4},{13,14,15,8,9,10,11,12},{21,22,23,16,17,18,19,20},{29..., dimensions={0} | all-to-all | bytes 65536 | tf_op jit(solution)/shard_map/all_to_all | solution.py:249
  19.9 0.0 collective-permute-done.1.sent_ref
  19.9 1.0 %shard_map.123 = (bf16[8,160,128]{2,1,0:T(8,128)(2,1)S(1)}, f32[512,128]{1,0:T(8,128)S(1)}, f32[32,128]{1,0:T(8,128)S(1)}, bf16[512,128]{1,0:T(8,128)(2,1)S(1)}, bf16[512,128]{1,0:T(8,128)(2,1)S(1)}) custom-call(f32[8,8,128]{2,1,0:T(8,128)S(1)} %all_to_all.15.all_sums, f32[512,128]{1,0:T(8,128)S(1)} %get-tuple-element.37.centered_ref, ...), custom_call_target="tpu_custom_call" | custom-call | flops 67108864 | tf_op jit(solution)/shard_map/pallas_call | solution.py:266
  20.9 21.6 %all_to_all.16.in_ref = bf16[8,160,128]{2,1,0:T(8,128)(2,1)S(1)} all-to-all(bf16[8,160,128]{2,1,0:T(8,128)(2,1)S(1)} %get-tuple-element.53), channel_id=1, replica_groups={{32,40,48,56,0,8,16,24},{33,41,49,57,1,9,17,25},{34,42,50,58,2,10,18,26..., dimensions={0} | all-to-all | bytes 655360 | tf_op jit(solution)/shard_map/all_to_all | solution.py:249
  42.5 0.7 %shard_map.125 = bf16[16,40,128]{2,1,0:T(8,128)(2,1)} custom-call(bf16[8,160,128]{2,1,0:T(8,128)(2,1)S(1)} %all_to_all.16.in_ref), custom_call_target="tpu_custom_call" | custom-call | flops 4194304 | tf_op jit(solution)/shard_map/pallas_call | solution.py:266
  43.2 18.2 %all-to-all-start.2 = ((bf16[16,40,128]{2,1,0:T(8,128)(2,1)}), bf16[16,40,128]{2,1,0:T(8,128)(2,1)S(1)}, u32[]{:S(2)}, u32[]{:S(2)}) async-start(bf16[16,40,128]{2,1,0:T(8,128)(2,1)} %shard_map.125), calls=%async_computation.2 | async-start | bytes 327680 | tf_op jit(solution)/shard_map/all_to_all | solution.py:249
  61.4 3.4 %collective-permute-start.2 = (f32[32,128]{1,0:T(8,128)S(1)}, f32[32,128]{1,0:T(8,128)S(1)}, u32[]{:S(2)}, u32[]{:S(2)}) collective-permute-start(f32[32,128]{1,0:T(8,128)S(1)} %get-tuple-element.50), channel_id=1, source_target_pairs={{8,0},{16,8},{24,16},{32,24},{40,32},{48,40},{56,48},{64,56},{72,6... | collective-permute-start | bytes 49160 | tf_op jit(solution)/shard_map/ppermute | solution.py:241
  64.9 5.3 %collective-permute-done.2.after_ref = f32[32,128]{1,0:T(8,128)S(1)} collective-permute-done((f32[32,128]{1,0:T(8,128)S(1)}, f32[32,128]{1,0:T(8,128)S(1)}, u32[]{:S(2)}, u32[]{:S(2)}) %collective-permute-start.2) | collective-permute-done | bytes 16416 | tf_op jit(solution)/shard_map/ppermute | solution.py:241
  70.2 1.3 %shard_map.124 = (bf16[512,128]{1,0:T(8,128)(2,1)}, bf16[512,128]{1,0:T(8,128)(2,1)}) custom-call(bf16[512,128]{1,0:T(8,128)(2,1)S(1)} %get-tuple-element.47.value_ref, bf16[512,128]{1,0:T(8,128)(2,1)S(1)} %get-tuple-element.48.gate_ref, f32[512,128]{1,0:T(8,128)S(1)} %get-tuple-element.49.conv_grad_ref, f32[32,128]{1,0:T(8,128)S(1)} %collective-permute-done.2.after_ref, ...), custom_call_target="tpu_custom_call" | custom-call | flops 268435456 | tf_op jit(solution)/shard_map/pallas_call | solution.py:266
  71.5 0.0 all-to-all-done.2.in_ref
  71.5 0.6 shard_map.126
Async XLA Ops:
  0.6 4.5 %copy-start.3 = (bf16[512,128]{1,0:T(8,128)(2,1)S(1)}, bf16[512,128]{1,0:T(8,128)(2,1)}, u32[]{:S(2)}) copy-start(bf16[512,128]{1,0:T(8,128)(2,1)} %gate_in.1) | copy-start | bytes 393220
  0.6 4.5 %copy-start.2 = (bf16[512,128]{1,0:T(8,128)(2,1)S(1)}, bf16[512,128]{1,0:T(8,128)(2,1)}, u32[]{:S(2)}) copy-start(bf16[512,128]{1,0:T(8,128)(2,1)} %value_in.1) | copy-start | bytes 393220
  0.7 4.5 %copy-start = (bf16[512,2048]{1,0:T(8,128)(2,1)S(1)}, bf16[512,2048]{1,0:T(8,128)(2,1)}, u32[]{:S(2)}) copy-start(bf16[512,2048]{1,0:T(8,128)(2,1)} %out_grad_ref.3) | copy-start | bytes 6291460
  0.7 4.5 %copy-start.4 = (f32[512]{0:T(512)S(1)}, f32[512]{0:T(512)}, u32[]{:S(2)}) copy-start(f32[512]{0:T(512)} %param.14) | copy-start | bytes 6148
  0.7 4.5 %copy-start.6 = (f32[512]{0:T(512)S(1)}, f32[512]{0:T(512)}, u32[]{:S(2)}) copy-start(f32[512]{0:T(512)} %param.13) | copy-start | bytes 6148
  0.7 4.5 %copy-start.1 = (bf16[2048,128]{1,0:T(8,128)(2,1)S(1)}, bf16[2048,128]{1,0:T(8,128)(2,1)}, u32[]{:S(2)}) copy-start(bf16[2048,128]{1,0:T(8,128)(2,1)} %weight_ref.1) | copy-start | bytes 1572868
  0.7 4.5 %copy-start.7 = (f32[128]{0:T(128)S(1)}, f32[128]{0:T(128)}, u32[]{:S(2)}) copy-start(f32[128]{0:T(128)} %param.11) | copy-start | bytes 1540
  0.7 4.5 %copy-start.5 = (bf16[31,128]{1,0:T(8,128)(2,1)S(1)}, bf16[31,128]{1,0:T(8,128)(2,1)}, u32[]{:S(2)}) copy-start(bf16[31,128]{1,0:T(8,128)(2,1)} %taps_raw.1) | copy-start | bytes 23812
  1.6 5.5 %collective-permute-start = (bf16[32,128]{1,0:T(8,128)(2,1)S(1)}, bf16[32,128]{1,0:T(8,128)(2,1)S(1)}, u32[]{:S(2)}, u32[]{:S(2)}) collective-permute-start(bf16[32,128]{1,0:T(8,128)(2,1)S(1)} %shard_map.119), channel_id=1, source_target_pairs={{0,8},{8,16},{16,24},{24,32},{32,40},{40,48},{48,56},{56,64},{64,7... | collective-permute-start | bytes 24584 | tf_op jit(solution)/shard_map/ppermute | solution.py:241
  8.2 11.7 %collective-permute-start.1 = (bf16[8,128,128]{2,1,0:T(8,128)(2,1)S(1)}, bf16[8,128,128]{2,1,0:T(8,128)(2,1)S(1)}, u32[]{:S(2)}, u32[]{:S(2)}) collective-permute-start(bf16[8,128,128]{2,1,0:T(8,128)(2,1)S(1)} %get-tuple-element.45), channel_id=1, source_target_pairs={{0,64},{64,0},{128,192},{192,128},{256,320},{320,256},{384,448},{4... | collective-permute-start | bytes 786440 | tf_op jit(solution)/shard_map/ppermute | solution.py:318
  43.2 28.3 %all-to-all-start.2 = ((bf16[16,40,128]{2,1,0:T(8,128)(2,1)}), bf16[16,40,128]{2,1,0:T(8,128)(2,1)S(1)}, u32[]{:S(2)}, u32[]{:S(2)}) async-start(bf16[16,40,128]{2,1,0:T(8,128)(2,1)} %shard_map.125), calls=%async_computation.2 | async-start | bytes 327680 | tf_op jit(solution)/shard_map/all_to_all | solution.py:249
  61.4 8.8 %collective-permute-start.2 = (f32[32,128]{1,0:T(8,128)S(1)}, f32[32,128]{1,0:T(8,128)S(1)}, u32[]{:S(2)}, u32[]{:S(2)}) collective-permute-start(f32[32,128]{1,0:T(8,128)S(1)} %get-tuple-element.50), channel_id=1, source_target_pairs={{8,0},{16,8},{24,16},{32,24},{40,32},{48,40},{56,48},{64,56},{72,6... | collective-permute-start | bytes 49160 | tf_op jit(solution)/shard_map/ppermute | solution.py:241

commit v6 on v5

--- a/solution.py
+++ b/solution.py
@@ -12,7 +12,7 @@
 HALO = 32
 BLOCK = 64
 LANES = 128
-Z_FIRST, Y_FIRST, TP_FIRST = 9, 4, 5
+Z_FIRST, Y_FIRST, TP_FIRST = 12, 5, 5
 F32, BF16 = jnp.float32, jnp.bfloat16
 VMEM = pl.BlockSpec(memory_space=pltpu.VMEM)
 HBM = pl.BlockSpec(memory_space=pltpu.HBM)
@@ -221,18 +221,46 @@
     gain_ref[...] = small[taps_n : taps_n + 1]
 
 
-def glu_kernel(
-    value_ref, gate_ref, conv_grad_ref, after_ref, taps, value_grad, gate_grad, padded
-):
-    rows, taps_n = value_ref.shape[0], taps.shape[0] - 1
-    padded[0:rows, :] = conv_grad_ref[...]
-    padded[rows : rows + HALO, :] = after_ref[...]
+def glu_block(value_ref, gate_ref, taps, padded, at, first, rows):
+    gated_grad = weighted(taps, padded, first + taps.shape[0] - 2, rows, -1)
+    sig = jax.nn.sigmoid(gate_ref[at : at + rows, :].astype(F32))
+    value = value_ref[at : at + rows, :].astype(F32)
+    return (gated_grad * sig).astype(BF16), (gated_grad * value * sig * (1.0 - sig)).astype(BF16)
+
+
+def glu_kernel(value_ref, gate_ref, conv_grad_ref, taps, value_out, gate_out, value_grad, gate_grad, sems):
+    rows = value_ref.shape[0] - HALO
+    copies = [
+        pltpu.make_async_copy(src.at[pl.ds(0, rows)], dst.at[pl.ds(0, rows)], sems.at[i])
+        for i, (src, dst) in enumerate(((value_grad, value_out), (gate_grad, gate_out)))
+    ]
     for r in range(0, rows, BLOCK):
-        gated_grad = weighted(taps, padded, r + taps_n - 1, BLOCK, -1)
-        sig = jax.nn.sigmoid(gate_ref[r : r + BLOCK, :].astype(F32))
-        value = value_ref[r : r + BLOCK, :].astype(F32)
-        value_grad[r : r + BLOCK, :] = (gated_grad * sig).astype(BF16)
-        gate_grad[r : r + BLOCK, :] = (gated_grad * value * sig * (1.0 - sig)).astype(BF16)
+        n = min(BLOCK, rows - r)
+        value_grad[r : r + n, :], gate_grad[r : r + n, :] = glu_block(
+            value_ref, gate_ref, taps, conv_grad_ref, r, r, n
+        )
+    for c in copies:
+        c.start()
+    for c in copies:
+        c.wait()
+
+
+def glu_end_kernel(
+    value_ref, gate_ref, conv_grad_ref, after_ref, taps, value_in, gate_in, value_out, gate_out,
+    padded, value_grad, gate_grad, sems,
+):
+    rows = value_ref.shape[0] - HALO
+    copies = [
+        pltpu.make_async_copy(src, dst.at[pl.ds(rows, HALO)], sems.at[i])
+        for i, (src, dst) in enumerate(((value_grad, value_out), (gate_grad, gate_out)))
+    ]
+    padded[0:HALO, :] = conv_grad_ref[rows:, :]
+    padded[HALO:, :] = after_ref[...]
+    value_grad[...], gate_grad[...] = glu_block(value_ref, gate_ref, taps, padded, rows, 0, HALO)
+    for c in copies:
+        c.start()
+    for c in copies:
+        c.wait()
 
 
 def passed_along(value, axis, by):
@@ -251,12 +279,13 @@
     )
 
 
-def call(kernel, outs, in_specs, scratch=(), flops=0, final=False):
+def call(kernel, outs, in_specs, scratch=(), flops=0, final=False, out_spec=VMEM, aliases=None):
     run = pl.pallas_call(
         kernel,
         out_shape=[jax.ShapeDtypeStruct(*o) if final else pltpu.VMEM(*o) for o in outs],
         in_specs=in_specs,
-        out_specs=[VMEM] * len(outs),
+        out_specs=[out_spec] * len(outs),
+        input_output_aliases=aliases or {},
         scratch_shapes=list(scratch),
         cost_estimate=pl.CostEstimate(flops=flops, bytes_accessed=0, transcendentals=0),
         compiler_params=pltpu.CompilerParams(vmem_limit_bytes=16 << 20),
@@ -334,9 +363,16 @@
     packed = exchange(packed, "z", order_z)
     after = passed_along(first_rows, SP, -1)
     value_grad, gate_grad = call(
-        glu_kernel, [(full, BF16), (full, BF16)], [VMEM] * 5,
-        [pltpu.VMEM((rows + HALO, chans), F32)], flops=1 << 28, final=True,
-    )(value, gate, conv_grad, after, taps)
+        glu_kernel, [(full, BF16), (full, BF16)], [VMEM] * 4,
+        [pltpu.VMEM(full, BF16), pltpu.VMEM(full, BF16), pltpu.SemaphoreType.DMA((2,))],
+        flops=1 << 28, final=True, out_spec=HBM,
+    )(value, gate, conv_grad, taps)
+    value_grad, gate_grad = call(
+        glu_end_kernel, [(full, BF16), (full, BF16)], [VMEM] * 5 + [HBM] * 2,
+        [pltpu.VMEM((2 * HALO, chans), F32), pltpu.VMEM(few, BF16), pltpu.VMEM(few, BF16),
+         pltpu.SemaphoreType.DMA((2,))],
+        flops=1 << 24, final=True, out_spec=HBM, aliases={5: 0, 6: 1},
+    )(value, gate, conv_grad, after, taps, value_grad, gate_grad)
     weight_grad, taps_grad, gain_grad = call(
         functools.partial(last_kernel, order=order_z),
         [((own, chans), F32), ((taps_n, chans), F32), ((1, chans), F32)], [VMEM], flops=1 << 22,

time: 72.6 us -> 70.1 us (0.966)
  the two profiles are of different devices: /device:TPU:56 before, /device:TPU:8 now
where the time goes in v6:
time: 70.1 us; the launch traced here: 69.7 us
  blocking collectives  21.8 us (31%)
  starting transfers between devices  21.7 us (31%)
  waiting for transfers between devices  17.5 us (25%)
  Pallas kernels  7.77 us (11%)
  between operations  0.83 us (1%)
    all_to_all x2, blocking collectives, exchange(): lax.all_to_all(value, axis, split_axis=0, concat_axis=0, tiled=True, axis...  21.8 us
    all_to_all x1, starting transfers between devices, exchange(): lax.all_to_all(value, axis, split_axis=0, concat_axis=0, tiled=True, axis...  13.2 us
    ppermute x2, waiting for transfers between devices, passed_along(): return lax.ppermute(value, axis, pairs)  12 us
    pallas_call x9, Pallas kernels, with_operands(): run(*(pltpu.with_memory_space_constraint(x, spec.memory_space) for x, spe...  7.77 us
    ppermute x2, starting transfers between devices, passed_along(): return lax.ppermute(value, axis, pairs)  6.59 us
    all_to_all x1, waiting for transfers between devices, exchange(): lax.all_to_all(value, axis, split_axis=0, concat_axis=0, tiled=True, axis...  5.46 us
    ppermute x1, starting transfers between devices, per_device(): sent = lax.ppermute(send, 'z', [(i, i ^ 1) for i in range(n_z)])  1.92 us
  transfers between devices with their start and end apart: 4, of which 3 were waited for; matrix products, arithmetic and copies ran while one was open for 0% of the time, Pallas kernels for 5%

profile of v6, /device:TPU:8, one launch (start us, length us, event | category | flops | bytes accessed | tf_op | source)
XLA Modules:
  0.0 69.7 jit_solution(1295814471198048723)
XLA Ops:
  0.6 0.0 copy-start.3
  0.6 0.0 copy-start.2
  0.7 0.0 copy-start
  0.7 0.0 copy-start.4
  0.7 0.0 copy-start.6
  0.7 0.0 copy-start.1
  0.7 0.0 copy-start.7
  0.7 0.0 copy-start.5
  0.7 0.9 %shard_map.119 = bf16[32,128]{1,0:T(8,128)(2,1)S(1)} custom-call(bf16[512,128]{1,0:T(8,128)(2,1)} %value_in.1, bf16[512,128]{1,0:T(8,128)(2,1)} %gate_in.1), custom_call_target="tpu_custom_call" | custom-call | flops 1073741824 | tf_op jit(solution)/shard_map/pallas_call | solution.py:295
  1.6 3.5 %collective-permute-start = (bf16[32,128]{1,0:T(8,128)(2,1)S(1)}, bf16[32,128]{1,0:T(8,128)(2,1)S(1)}, u32[]{:S(2)}, u32[]{:S(2)}) collective-permute-start(bf16[32,128]{1,0:T(8,128)(2,1)S(1)} %shard_map.119), channel_id=1, source_target_pairs={{0,8},{8,16},{16,24},{24,32},{32,40},{40,48},{48,56},{56,64},{64,7... | collective-permute-start | bytes 24584 | tf_op jit(solution)/shard_map/ppermute | solution.py:269
  5.1 0.0 copy-done.3
  5.1 0.0 copy-done.2
  5.1 0.0 copy-done
  5.1 0.0 copy-done.4
  5.2 0.0 copy-done.6
  5.2 0.0 copy-done.1
  5.2 0.0 copy-done.7
  5.2 0.0 copy-done.5
  5.2 1.6 %shard_map.120 = (f32[32,128]{1,0:T(8,128)S(1)}, bf16[512,128]{1,0:T(8,128)(2,1)S(1)}, f32[512,128]{1,0:T(8,128)S(1)}, f32[512,128]{1,0:T(8,128)S(1)}, bf16[512,...) custom-call(bf16[512,128]{1,0:T(8,128)(2,1)S(1)} %copy-done.2, ...), custom_call_target="tpu_custom_call" | custom-call | flops 268435456 | tf_op jit(solution)/shard_map/pallas_call | solution.py:295
  6.8 10.8 %collective-permute-done.before_ref = bf16[32,128]{1,0:T(8,128)(2,1)S(1)} collective-permute-done((bf16[32,128]{1,0:T(8,128)(2,1)S(1)}, bf16[32,128]{1,0:T(8,128)(2,1)S(1)}, u32[]{:S(2)}, u32[]{:S(2)}) %collective-permute-start) | collective-permute-done | bytes 8224 | tf_op jit(solution)/shard_map/ppermute | solution.py:269
  17.6 0.2 shard_map.121
  17.8 0.8 %shard_map.122 = (f32[8,128,128]{2,1,0:T(8,128)S(1)}, bf16[8,128,128]{2,1,0:T(8,128)(2,1)S(1)}) custom-call(bf16[512,2048]{1,0:T(8,128)(2,1)S(1)} %copy-done, bf16[512,128]{1,0:T(8,128)(2,1)S(1)} %get-tuple-element.44.activated_ref, bf16[32,128]{1,0:T(8,128)(2,1)S(1)} %get-tuple-element.45.activated_first), custom_call_target="tpu_custom_call" | custom-call | flops 268435456 | tf_op jit(solution)/shard_map/pallas_call | solution.py:295
  18.6 1.9 %collective-permute-start.1 = (bf16[8,128,128]{2,1,0:T(8,128)(2,1)S(1)}, bf16[8,128,128]{2,1,0:T(8,128)(2,1)S(1)}, u32[]{:S(2)}, u32[]{:S(2)}) collective-permute-start(bf16[8,128,128]{2,1,0:T(8,128)(2,1)S(1)} %get-tuple-element.47), channel_id=1, source_target_pairs={{0,64},{64,0},{128,192},{192,128},{256,320},{320,256},{384,448},{4... | collective-permute-start | bytes 786440 | tf_op jit(solution)/shard_map/ppermute | solution.py:347
  20.5 6.7 %all_to_all.15.all_sums = f32[8,8,128]{2,1,0:T(8,128)S(1)} all-to-all(f32[8,8,128]{2,1,0:T(8,128)S(1)} %get-tuple-element.38), channel_id=1, replica_groups={{5,6,7,0,1,2,3,4},{13,14,15,8,9,10,11,12},{21,22,23,16,17,18,19,20},{29..., dimensions={0} | all-to-all | bytes 65536 | tf_op jit(solution)/shard_map/all_to_all | solution.py:277
  27.3 0.0 collective-permute-done.1.sent_ref
  27.3 1.0 %shard_map.123 = (bf16[8,160,128]{2,1,0:T(8,128)(2,1)S(1)}, f32[512,128]{1,0:T(8,128)S(1)}, f32[32,128]{1,0:T(8,128)S(1)}, bf16[512,128]{1,0:T(8,128)(2,1)S(1)}, bf16[512,128]{1,0:T(8,128)(2,1)S(1)}) custom-call(f32[8,8,128]{2,1,0:T(8,128)S(1)} %all_to_all.15.all_sums, f32[512,128]{1,0:T(8,128)S(1)} %get-tuple-element.39.centered_ref, ...), custom_call_target="tpu_custom_call" | custom-call | flops 67108864 | tf_op jit(solution)/shard_map/pallas_call | solution.py:295
  28.3 15.1 %all_to_all.16.in_ref = bf16[8,160,128]{2,1,0:T(8,128)(2,1)S(1)} all-to-all(bf16[8,160,128]{2,1,0:T(8,128)(2,1)S(1)} %get-tuple-element.57), channel_id=1, replica_groups={{40,48,56,0,8,16,24,32},{41,49,57,1,9,17,25,33},{42,50,58,2,10,18,26,34..., dimensions={0} | all-to-all | bytes 655360 | tf_op jit(solution)/shard_map/all_to_all | solution.py:277
  43.4 0.7 %shard_map.126 = bf16[16,40,128]{2,1,0:T(8,128)(2,1)} custom-call(bf16[8,160,128]{2,1,0:T(8,128)(2,1)S(1)} %all_to_all.16.in_ref), custom_call_target="tpu_custom_call" | custom-call | flops 4194304 | tf_op jit(solution)/shard_map/pallas_call | solution.py:295
  44.1 13.2 %all-to-all-start.2 = ((bf16[16,40,128]{2,1,0:T(8,128)(2,1)}), bf16[16,40,128]{2,1,0:T(8,128)(2,1)S(1)}, u32[]{:S(2)}, u32[]{:S(2)}) async-start(bf16[16,40,128]{2,1,0:T(8,128)(2,1)} %shard_map.126), calls=%async_computation.2 | async-start | bytes 327680 | tf_op jit(solution)/shard_map/all_to_all | solution.py:277
  57.3 3.1 %collective-permute-start.2 = (f32[32,128]{1,0:T(8,128)S(1)}, f32[32,128]{1,0:T(8,128)S(1)}, u32[]{:S(2)}, u32[]{:S(2)}) collective-permute-start(f32[32,128]{1,0:T(8,128)S(1)} %get-tuple-element.52), channel_id=1, source_target_pairs={{8,0},{16,8},{24,16},{32,24},{40,32},{48,40},{56,48},{64,56},{72,6... | collective-permute-start | bytes 49160 | tf_op jit(solution)/shard_map/ppermute | solution.py:269
  60.4 1.3 %shard_map.124 = (bf16[512,128]{1,0:T(8,128)(2,1)}, bf16[512,128]{1,0:T(8,128)(2,1)}) custom-call(bf16[512,128]{1,0:T(8,128)(2,1)S(1)} %get-tuple-element.49.value_ref, bf16[512,128]{1,0:T(8,128)(2,1)S(1)} %get-tuple-element.50.gate_ref, f32[512,128]{1,0:T(8,128)S(1)} %get-tuple-element.51.conv_grad_ref, f32[32,128]{1,0:T(8,128)S(1)} %get-tuple-element.35.taps), custom_call_target="tpu_custom_call" | custom-call | flops 268435456 | tf_op jit(solution)/shard_map/pallas_call | solution.py:295
  61.7 1.2 %collective-permute-done.2.after_ref = f32[32,128]{1,0:T(8,128)S(1)} collective-permute-done((f32[32,128]{1,0:T(8,128)S(1)}, f32[32,128]{1,0:T(8,128)S(1)}, u32[]{:S(2)}, u32[]{:S(2)}) %collective-permute-start.2) | collective-permute-done | bytes 16416 | tf_op jit(solution)/shard_map/ppermute | solution.py:269
  62.9 0.7 shard_map.125
  63.6 5.5 %all-to-all-done.2.in_ref = bf16[16,40,128]{2,1,0:T(8,128)(2,1)S(1)} async-done(((bf16[16,40,128]{2,1,0:T(8,128)(2,1)}), bf16[16,40,128]{2,1,0:T(8,128)(2,1)S(1)}, u32[]{:S(2)}, u32[]{:S(2)}) %all-to-all-start.2) | async-done | bytes 163872 | tf_op jit(solution)/shard_map/all_to_all | solution.py:277
  69.1 0.6 shard_map.127
Async XLA Ops:
  0.6 4.5 %copy-start.3 = (bf16[512,128]{1,0:T(8,128)(2,1)S(1)}, bf16[512,128]{1,0:T(8,128)(2,1)}, u32[]{:S(2)}) copy-start(bf16[512,128]{1,0:T(8,128)(2,1)} %gate_in.1) | copy-start | bytes 393220
  0.6 4.5 %copy-start.2 = (bf16[512,128]{1,0:T(8,128)(2,1)S(1)}, bf16[512,128]{1,0:T(8,128)(2,1)}, u32[]{:S(2)}) copy-start(bf16[512,128]{1,0:T(8,128)(2,1)} %value_in.1) | copy-start | bytes 393220
  0.7 4.5 %copy-start = (bf16[512,2048]{1,0:T(8,128)(2,1)S(1)}, bf16[512,2048]{1,0:T(8,128)(2,1)}, u32[]{:S(2)}) copy-start(bf16[512,2048]{1,0:T(8,128)(2,1)} %out_grad_ref.3) | copy-start | bytes 6291460
  0.7 4.5 %copy-start.4 = (f32[512]{0:T(512)S(1)}, f32[512]{0:T(512)}, u32[]{:S(2)}) copy-start(f32[512]{0:T(512)} %param.14) | copy-start | bytes 6148
  0.7 4.5 %copy-start.6 = (f32[512]{0:T(512)S(1)}, f32[512]{0:T(512)}, u32[]{:S(2)}) copy-start(f32[512]{0:T(512)} %param.13) | copy-start | bytes 6148
  0.7 4.5 %copy-start.1 = (bf16[2048,128]{1,0:T(8,128)(2,1)S(1)}, bf16[2048,128]{1,0:T(8,128)(2,1)}, u32[]{:S(2)}) copy-start(bf16[2048,128]{1,0:T(8,128)(2,1)} %weight_ref.1) | copy-start | bytes 1572868
  0.7 4.5 %copy-start.7 = (f32[128]{0:T(128)S(1)}, f32[128]{0:T(128)}, u32[]{:S(2)}) copy-start(f32[128]{0:T(128)} %param.11) | copy-start | bytes 1540
  0.7 4.5 %copy-start.5 = (bf16[31,128]{1,0:T(8,128)(2,1)S(1)}, bf16[31,128]{1,0:T(8,128)(2,1)}, u32[]{:S(2)}) copy-start(bf16[31,128]{1,0:T(8,128)(2,1)} %taps_raw.1) | copy-start | bytes 23812
  1.6 16.0 %collective-permute-start = (bf16[32,128]{1,0:T(8,128)(2,1)S(1)}, bf16[32,128]{1,0:T(8,128)(2,1)S(1)}, u32[]{:S(2)}, u32[]{:S(2)}) collective-permute-start(bf16[32,128]{1,0:T(8,128)(2,1)S(1)} %shard_map.119), channel_id=1, source_target_pairs={{0,8},{8,16},{16,24},{24,32},{32,40},{40,48},{48,56},{56,64},{64,7... | collective-permute-start | bytes 24584 | tf_op jit(solution)/shard_map/ppermute | solution.py:269
  18.6 8.7 %collective-permute-start.1 = (bf16[8,128,128]{2,1,0:T(8,128)(2,1)S(1)}, bf16[8,128,128]{2,1,0:T(8,128)(2,1)S(1)}, u32[]{:S(2)}, u32[]{:S(2)}) collective-permute-start(bf16[8,128,128]{2,1,0:T(8,128)(2,1)S(1)} %get-tuple-element.47), channel_id=1, source_target_pairs={{0,64},{64,0},{128,192},{192,128},{256,320},{320,256},{384,448},{4... | collective-permute-start | bytes 786440 | tf_op jit(solution)/shard_map/ppermute | solution.py:347
  44.1 25.0 %all-to-all-start.2 = ((bf16[16,40,128]{2,1,0:T(8,128)(2,1)}), bf16[16,40,128]{2,1,0:T(8,128)(2,1)S(1)}, u32[]{:S(2)}, u32[]{:S(2)}) async-start(bf16[16,40,128]{2,1,0:T(8,128)(2,1)} %shard_map.126), calls=%async_computation.2 | async-start | bytes 327680 | tf_op jit(solution)/shard_map/all_to_all | solution.py:277
  57.3 5.6 %collective-permute-start.2 = (f32[32,128]{1,0:T(8,128)S(1)}, f32[32,128]{1,0:T(8,128)S(1)}, u32[]{:S(2)}, u32[]{:S(2)}) collective-permute-start(f32[32,128]{1,0:T(8,128)S(1)} %get-tuple-element.52), channel_id=1, source_target_pairs={{8,0},{16,8},{24,16},{32,24},{40,32},{48,40},{56,48},{64,56},{72,6... | collective-permute-start | bytes 49160 | tf_op jit(solution)/shard_map/ppermute | solution.py:269

commit v7 on v6

--- a/solution.py
+++ b/solution.py
@@ -150,6 +150,22 @@
             send_ref[y, z * half : (z + 1) * half, :] = jnp.where(even, lower, upper).astype(BF16)
 
 
+def first_weight_kernel(
+    before_ref, conv_first, act_first, taps, gain_ref, mean_ref, scale_ref, gain_sum, sums_ref,
+    out_grad_ref, activated_ref,
+    centered_first, scaled_first, gain_out, sums_out, keep_ref, send_ref,
+    padded, activated_first,
+    *, n_z, n_y,
+):
+    first_kernel(
+        before_ref, conv_first, act_first, taps, gain_ref, mean_ref, scale_ref, gain_sum, sums_ref,
+        centered_first, scaled_first, activated_first, gain_out, sums_out, padded,
+    )
+    weight_kernel(
+        out_grad_ref, activated_ref, activated_first, keep_ref, send_ref, n_z=n_z, n_y=n_y
+    )
+
+
 def pack_kernel(
     all_sums, centered_ref, scaled_ref, centered_first, scaled_first, gated_ref, before_ref,
     scale_ref, keep_ref, sent_ref, gain_sum, value_in, gate_in,
@@ -332,18 +348,14 @@
         [pltpu.VMEM((HALO + rows, chans), F32), pltpu.VMEM(full, F32)],
         flops=1 << 28,
     )(glu_value, glu_gate, conv_taps, gain, mean, scale, out_weight, out_grad)
-    centered0, scaled0, activated0, gain_sum, sums = call(
-        first_kernel,
-        [(few, F32), (few, F32), (few, BF16), ((8, chans), F32), ((n_tp, 2 * n_b, LANES), F32)],
-        [VMEM] * 9,
-        [pltpu.VMEM((2 * HALO, chans), F32)],
-        flops=1 << 24,
-    )(before, conv0, act0, taps, gain, mean, scale, gain_sum, sums)
-    keep, send = call(
-        functools.partial(weight_kernel, n_z=n_z, n_y=n_y),
-        [((n_y, n_z * half, chans), F32), ((n_y, n_z * half, chans), BF16)],
-        [VMEM] * 3, flops=1 << 28,
-    )(out_grad, activated, activated0)
+    centered0, scaled0, gain_sum, sums, keep, send = call(
+        functools.partial(first_weight_kernel, n_z=n_z, n_y=n_y),
+        [(few, F32), (few, F32), ((8, chans), F32), ((n_tp, 2 * n_b, LANES), F32),
+         ((n_y, n_z * half, chans), F32), ((n_y, n_z * half, chans), BF16)],
+        [VMEM] * 11,
+        [pltpu.VMEM((2 * HALO, chans), F32), pltpu.VMEM(few, BF16)],
+        flops=1 << 28,
+    )(before, conv0, act0, taps, gain, mean, scale, gain_sum, sums, out_grad, activated)
     sent = lax.ppermute(send, "z", [(i, i ^ 1) for i in range(n_z)])
     sums = exchange(sums, "tp", order_tp)
     packed, conv_grad, first_rows, value, gate = call(

time: 70.1 us -> 70 us (level)
    pallas_call x9 -> x8, Pallas kernels: 7.77 us -> 7.63 us  [with_operands(): run(*(pltpu.with_memory_space_constraint(x, spec.memory_space) for x, spe...]
where the time goes in v7:
time: 70 us; the launch traced here: 69.6 us
  blocking collectives  21.8 us (31%)
  starting transfers between devices  21.7 us (31%)
  waiting for transfers between devices  17.5 us (25%)
  Pallas kernels  7.63 us (11%)
  between operations  0.83 us (1%)
    all_to_all x2, blocking collectives, exchange(): lax.all_to_all(value, axis, split_axis=0, concat_axis=0, tiled=True, axis...  21.8 us
    all_to_all x1, starting transfers between devices, exchange(): lax.all_to_all(value, axis, split_axis=0, concat_axis=0, tiled=True, axis...  13.2 us
    ppermute x2, waiting for transfers between devices, passed_along(): return lax.ppermute(value, axis, pairs)  12 us
    pallas_call x8, Pallas kernels, with_operands(): run(*(pltpu.with_memory_space_constraint(x, spec.memory_space) for x, spe...  7.63 us
    ppermute x2, starting transfers between devices, passed_along(): return lax.ppermute(value, axis, pairs)  6.59 us
    all_to_all x1, waiting for transfers between devices, exchange(): lax.all_to_all(value, axis, split_axis=0, concat_axis=0, tiled=True, axis...  5.46 us
    ppermute x1, starting transfers between devices, per_device(): sent = lax.ppermute(send, 'z', [(i, i ^ 1) for i in range(n_z)])  1.92 us
  transfers between devices with their start and end apart: 4, of which 3 were waited for; matrix products, arithmetic and copies ran while one was open for 0% of the time, Pallas kernels for 5%

profile of v7, /device:TPU:8, one launch (start us, length us, event | category | flops | bytes accessed | tf_op | source)
XLA Modules:
  0.0 69.6 jit_solution(6031095032677395314)
XLA Ops:
  0.6 0.0 copy-start.3
  0.6 0.0 copy-start.2
  0.7 0.0 copy-start
  0.7 0.0 copy-start.4
  0.7 0.0 copy-start.6
  0.7 0.0 copy-start.1
  0.7 0.0 copy-start.7
  0.7 0.0 copy-start.5
  0.7 0.9 %shard_map.119 = bf16[32,128]{1,0:T(8,128)(2,1)S(1)} custom-call(bf16[512,128]{1,0:T(8,128)(2,1)} %value_in.1, bf16[512,128]{1,0:T(8,128)(2,1)} %gate_in.1), custom_call_target="tpu_custom_call" | custom-call | flops 1073741824 | tf_op jit(solution)/shard_map/pallas_call | solution.py:311
  1.6 3.5 %collective-permute-start = (bf16[32,128]{1,0:T(8,128)(2,1)S(1)}, bf16[32,128]{1,0:T(8,128)(2,1)S(1)}, u32[]{:S(2)}, u32[]{:S(2)}) collective-permute-start(bf16[32,128]{1,0:T(8,128)(2,1)S(1)} %shard_map.119), channel_id=1, source_target_pairs={{0,8},{8,16},{16,24},{24,32},{32,40},{40,48},{48,56},{56,64},{64,7... | collective-permute-start | bytes 24584 | tf_op jit(solution)/shard_map/ppermute | solution.py:285
  5.1 0.0 copy-done.3
  5.1 0.0 copy-done.2
  5.1 0.0 copy-done
  5.1 0.0 copy-done.4
  5.2 0.0 copy-done.6
  5.2 0.0 copy-done.1
  5.2 0.0 copy-done.7
  5.2 0.0 copy-done.5
  5.2 1.6 %shard_map.120 = (f32[32,128]{1,0:T(8,128)S(1)}, bf16[512,128]{1,0:T(8,128)(2,1)S(1)}, f32[512,128]{1,0:T(8,128)S(1)}, f32[512,128]{1,0:T(8,128)S(1)}, bf16[512,...) custom-call(bf16[512,128]{1,0:T(8,128)(2,1)S(1)} %copy-done.2, ...), custom_call_target="tpu_custom_call" | custom-call | flops 268435456 | tf_op jit(solution)/shard_map/pallas_call | solution.py:311
  6.8 10.8 %collective-permute-done.before_ref = bf16[32,128]{1,0:T(8,128)(2,1)S(1)} collective-permute-done((bf16[32,128]{1,0:T(8,128)(2,1)S(1)}, bf16[32,128]{1,0:T(8,128)(2,1)S(1)}, u32[]{:S(2)}, u32[]{:S(2)}) %collective-permute-start) | collective-permute-done | bytes 8224 | tf_op jit(solution)/shard_map/ppermute | solution.py:285
  17.6 0.9 %shard_map.121 = (f32[32,128]{1,0:T(8,128)S(1)}, f32[32,128]{1,0:T(8,128)S(1)}, f32[8,128]{1,0:T(8,128)S(1)}, f32[8,8,128]{2,1,0:T(8,128)S(1)}, f32[8,128,128]{2...) custom-call(bf16[32,128]{1,0:T(8,128)(2,1)S(1)} %collective-permute-done.before_ref, ...), custom_call_target="tpu_custom_call" | custom-call | flops 268435456 | tf_op jit(solution)/shard_map/pallas_call | solution.py:311
  18.5 1.9 %collective-permute-start.1 = (bf16[8,128,128]{2,1,0:T(8,128)(2,1)S(1)}, bf16[8,128,128]{2,1,0:T(8,128)(2,1)S(1)}, u32[]{:S(2)}, u32[]{:S(2)}) collective-permute-start(bf16[8,128,128]{2,1,0:T(8,128)(2,1)S(1)} %get-tuple-element.45), channel_id=1, source_target_pairs={{0,64},{64,0},{128,192},{192,128},{256,320},{320,256},{384,448},{4... | collective-permute-start | bytes 786440 | tf_op jit(solution)/shard_map/ppermute | solution.py:359
  20.4 6.7 %all_to_all.15.all_sums = f32[8,8,128]{2,1,0:T(8,128)S(1)} all-to-all(f32[8,8,128]{2,1,0:T(8,128)S(1)} %get-tuple-element.38), channel_id=1, replica_groups={{5,6,7,0,1,2,3,4},{13,14,15,8,9,10,11,12},{21,22,23,16,17,18,19,20},{29..., dimensions={0} | all-to-all | bytes 65536 | tf_op jit(solution)/shard_map/all_to_all | solution.py:293
  27.1 0.0 collective-permute-done.1.sent_ref
  27.1 1.0 %shard_map.122 = (bf16[8,160,128]{2,1,0:T(8,128)(2,1)S(1)}, f32[512,128]{1,0:T(8,128)S(1)}, f32[32,128]{1,0:T(8,128)S(1)}, bf16[512,128]{1,0:T(8,128)(2,1)S(1)}, bf16[512,128]{1,0:T(8,128)(2,1)S(1)}) custom-call(f32[8,8,128]{2,1,0:T(8,128)S(1)} %all_to_all.15.all_sums, f32[512,128]{1,0:T(8,128)S(1)} %get-tuple-element.39.centered_ref, ...), custom_call_target="tpu_custom_call" | custom-call | flops 67108864 | tf_op jit(solution)/shard_map/pallas_call | solution.py:311
  28.1 15.1 %all_to_all.16.in_ref = bf16[8,160,128]{2,1,0:T(8,128)(2,1)S(1)} all-to-all(bf16[8,160,128]{2,1,0:T(8,128)(2,1)S(1)} %get-tuple-element.55), channel_id=1, replica_groups={{40,48,56,0,8,16,24,32},{41,49,57,1,9,17,25,33},{42,50,58,2,10,18,26,34..., dimensions={0} | all-to-all | bytes 655360 | tf_op jit(solution)/shard_map/all_to_all | solution.py:293
  43.2 0.7 %shard_map.125 = bf16[16,40,128]{2,1,0:T(8,128)(2,1)} custom-call(bf16[8,160,128]{2,1,0:T(8,128)(2,1)S(1)} %all_to_all.16.in_ref), custom_call_target="tpu_custom_call" | custom-call | flops 4194304 | tf_op jit(solution)/shard_map/pallas_call | solution.py:311
  43.9 13.2 %all-to-all-start.2 = ((bf16[16,40,128]{2,1,0:T(8,128)(2,1)}), bf16[16,40,128]{2,1,0:T(8,128)(2,1)S(1)}, u32[]{:S(2)}, u32[]{:S(2)}) async-start(bf16[16,40,128]{2,1,0:T(8,128)(2,1)} %shard_map.125), calls=%async_computation.2 | async-start | bytes 327680 | tf_op jit(solution)/shard_map/all_to_all | solution.py:293
  57.2 3.1 %collective-permute-start.2 = (f32[32,128]{1,0:T(8,128)S(1)}, f32[32,128]{1,0:T(8,128)S(1)}, u32[]{:S(2)}, u32[]{:S(2)}) collective-permute-start(f32[32,128]{1,0:T(8,128)S(1)} %get-tuple-element.50), channel_id=1, source_target_pairs={{8,0},{16,8},{24,16},{32,24},{40,32},{48,40},{56,48},{64,56},{72,6... | collective-permute-start | bytes 49160 | tf_op jit(solution)/shard_map/ppermute | solution.py:285
  60.3 1.3 %shard_map.123 = (bf16[512,128]{1,0:T(8,128)(2,1)}, bf16[512,128]{1,0:T(8,128)(2,1)}) custom-call(bf16[512,128]{1,0:T(8,128)(2,1)S(1)} %get-tuple-element.47.value_ref, bf16[512,128]{1,0:T(8,128)(2,1)S(1)} %get-tuple-element.48.gate_ref, f32[512,128]{1,0:T(8,128)S(1)} %get-tuple-element.49.conv_grad_ref, f32[32,128]{1,0:T(8,128)S(1)} %get-tuple-element.34.taps), custom_call_target="tpu_custom_call" | custom-call | flops 268435456 | tf_op jit(solution)/shard_map/pallas_call | solution.py:311
  61.6 1.2 %collective-permute-done.2.after_ref = f32[32,128]{1,0:T(8,128)S(1)} collective-permute-done((f32[32,128]{1,0:T(8,128)S(1)}, f32[32,128]{1,0:T(8,128)S(1)}, u32[]{:S(2)}, u32[]{:S(2)}) %collective-permute-start.2) | collective-permute-done | bytes 16416 | tf_op jit(solution)/shard_map/ppermute | solution.py:285
  62.8 0.7 shard_map.124
  63.5 5.5 %all-to-all-done.2.in_ref = bf16[16,40,128]{2,1,0:T(8,128)(2,1)S(1)} async-done(((bf16[16,40,128]{2,1,0:T(8,128)(2,1)}), bf16[16,40,128]{2,1,0:T(8,128)(2,1)S(1)}, u32[]{:S(2)}, u32[]{:S(2)}) %all-to-all-start.2) | async-done | bytes 163872 | tf_op jit(solution)/shard_map/all_to_all | solution.py:293
  68.9 0.6 shard_map.126
Async XLA Ops:
  0.6 4.5 %copy-start.3 = (bf16[512,128]{1,0:T(8,128)(2,1)S(1)}, bf16[512,128]{1,0:T(8,128)(2,1)}, u32[]{:S(2)}) copy-start(bf16[512,128]{1,0:T(8,128)(2,1)} %gate_in.1) | copy-start | bytes 393220
  0.6 4.5 %copy-start.2 = (bf16[512,128]{1,0:T(8,128)(2,1)S(1)}, bf16[512,128]{1,0:T(8,128)(2,1)}, u32[]{:S(2)}) copy-start(bf16[512,128]{1,0:T(8,128)(2,1)} %value_in.1) | copy-start | bytes 393220
  0.7 4.5 %copy-start = (bf16[512,2048]{1,0:T(8,128)(2,1)S(1)}, bf16[512,2048]{1,0:T(8,128)(2,1)}, u32[]{:S(2)}) copy-start(bf16[512,2048]{1,0:T(8,128)(2,1)} %out_grad_ref.3) | copy-start | bytes 6291460
  0.7 4.5 %copy-start.4 = (f32[512]{0:T(512)S(1)}, f32[512]{0:T(512)}, u32[]{:S(2)}) copy-start(f32[512]{0:T(512)} %param.14) | copy-start | bytes 6148
  0.7 4.5 %copy-start.6 = (f32[512]{0:T(512)S(1)}, f32[512]{0:T(512)}, u32[]{:S(2)}) copy-start(f32[512]{0:T(512)} %param.13) | copy-start | bytes 6148
  0.7 4.5 %copy-start.1 = (bf16[2048,128]{1,0:T(8,128)(2,1)S(1)}, bf16[2048,128]{1,0:T(8,128)(2,1)}, u32[]{:S(2)}) copy-start(bf16[2048,128]{1,0:T(8,128)(2,1)} %weight_ref.1) | copy-start | bytes 1572868
  0.7 4.5 %copy-start.7 = (f32[128]{0:T(128)S(1)}, f32[128]{0:T(128)}, u32[]{:S(2)}) copy-start(f32[128]{0:T(128)} %param.11) | copy-start | bytes 1540
  0.7 4.5 %copy-start.5 = (bf16[31,128]{1,0:T(8,128)(2,1)S(1)}, bf16[31,128]{1,0:T(8,128)(2,1)}, u32[]{:S(2)}) copy-start(bf16[31,128]{1,0:T(8,128)(2,1)} %taps_raw.1) | copy-start | bytes 23812
  1.6 16.0 %collective-permute-start = (bf16[32,128]{1,0:T(8,128)(2,1)S(1)}, bf16[32,128]{1,0:T(8,128)(2,1)S(1)}, u32[]{:S(2)}, u32[]{:S(2)}) collective-permute-start(bf16[32,128]{1,0:T(8,128)(2,1)S(1)} %shard_map.119), channel_id=1, source_target_pairs={{0,8},{8,16},{16,24},{24,32},{32,40},{40,48},{48,56},{56,64},{64,7... | collective-permute-start | bytes 24584 | tf_op jit(solution)/shard_map/ppermute | solution.py:285
  18.5 8.7 %collective-permute-start.1 = (bf16[8,128,128]{2,1,0:T(8,128)(2,1)S(1)}, bf16[8,128,128]{2,1,0:T(8,128)(2,1)S(1)}, u32[]{:S(2)}, u32[]{:S(2)}) collective-permute-start(bf16[8,128,128]{2,1,0:T(8,128)(2,1)S(1)} %get-tuple-element.45), channel_id=1, source_target_pairs={{0,64},{64,0},{128,192},{192,128},{256,320},{320,256},{384,448},{4... | collective-permute-start | bytes 786440 | tf_op jit(solution)/shard_map/ppermute | solution.py:359
  43.9 25.0 %all-to-all-start.2 = ((bf16[16,40,128]{2,1,0:T(8,128)(2,1)}), bf16[16,40,128]{2,1,0:T(8,128)(2,1)S(1)}, u32[]{:S(2)}, u32[]{:S(2)}) async-start(bf16[16,40,128]{2,1,0:T(8,128)(2,1)} %shard_map.125), calls=%async_computation.2 | async-start | bytes 327680 | tf_op jit(solution)/shard_map/all_to_all | solution.py:293
  57.2 5.6 %collective-permute-start.2 = (f32[32,128]{1,0:T(8,128)S(1)}, f32[32,128]{1,0:T(8,128)S(1)}, u32[]{:S(2)}, u32[]{:S(2)}) collective-permute-start(f32[32,128]{1,0:T(8,128)S(1)} %get-tuple-element.50), channel_id=1, source_target_pairs={{8,0},{16,8},{24,16},{32,24},{40,32},{48,40},{56,48},{64,56},{72,6... | collective-permute-start | bytes 49160 | tf_op jit(solution)/shard_map/ppermute | solution.py:285
